TPU v7x, 32 devices: a whole 2x2x4 slice. The times are simulated.
32 devices in a mesh: grp: 2 (over y), sp: 4 (over z), tp: 4 (over x, core).
Axes of the slice: x: 2, y: 2, z: 4, core: 2. Of those that a mesh axis runs over, the one named last changes fastest.
Arguments:
- inputs: bfloat16 [2048, 2048], P(('grp', 'sp'), 'tp'), parts along dimension 0, may hold values from -20 to 20
- norm_gain: bfloat16 [2048], replicated, may hold values from 0.099609375 to 1.8984375
- w_conv_in: bfloat16 [1024, 2048], P('tp'), may hold values from -0.125 to 0.125
- w_conv_gate: bfloat16 [1024, 2048], P('tp'), may hold values from -0.125 to 0.125
- conv_kernel: bfloat16 [31, 1024], P(None, 'tp'), may hold values from -4.3105272 to 4.3105272
- ln_gain: bfloat16 [1024], P('tp'), may hold values from 0.099609375 to 1.8984375
- w_query: bfloat16 [1024, 2048], P('tp'), may hold values from -0.53033009 to 0.53033009
- w_key: bfloat16 [1024, 2048], P('tp'), may hold values from -0.53033009 to 0.53033009
- w_value: bfloat16 [1024, 2048], P('tp'), may hold values from -0.125 to 0.125
- cum_gate: float32 [16, 2048], P('tp', ('grp', 'sp')), parts along dimension 1, may hold values from -1024 to 0, as said below
- w_conv_out: bfloat16 [1024, 2048], P('tp'), may hold values from -0.125 to 0.125
- w_attn_out: bfloat16 [1024, 2048], P('tp'), may hold values from -0.125 to 0.125
Outputs:
- mixed: bfloat16 [2048, 2048], P(('grp', 'sp', 'tp')), parts along dimension 0
- log_total: float32 [16, 2048], P('tp', ('grp', 'sp')), parts along dimension 1
There are 2 independent parts, one for each index of `grp`. A program takes and returns all parts, laid end to end along the dimension named above; an argument that names none is the same for every part. Nothing has to cross between parts.
Inputs may be any that keep to these rules, and one draw needn't show every extreme that they name: cum_gate never rises along positions: entry t is the sum of the head's log forget gates at positions 0 to t.
All inputs are finite; a program needn't handle non-finite values.
Results may differ from a plain program's by a relative error of at most 0.0144.
Values may be sent and summed in bfloat16 or wider, within the bound.
A program may use at most 64 MiB of HBM per device.

v0:
```python
import functools
import jax
import jax.numpy as jnp
from jax import lax
from jax.experimental import pallas as pl
from jax.experimental.pallas import tpu as pltpu
from jax.sharding import PartitionSpec as P

D = 2048
CONV_CH = 1024
HEADS = 16


neg_large = -1e30


def passed_along(block, axis, distance):
    devices = range(lax.axis_size(axis))
    route = [(i - distance, i) for i in devices if i - distance in devices]
    return lax.ppermute(block, axis, route)


def block_terms(q_blk, q_cum, k_blk, v_blk, k_cum, q_first, k_first):
    score_scale = q_blk.shape[2] ** (-0.5)
    scores = (
        jnp.einsum("qhd,khd->hqk", q_blk, k_blk, preferred_element_type=jnp.float32) * score_scale
    )
    scores = scores + q_cum[:, :, None] - k_cum[:, None, :]
    q_pos = q_first + jnp.arange(q_blk.shape[0], dtype=jnp.int32)
    k_pos = k_first + jnp.arange(k_blk.shape[0], dtype=jnp.int32)
    allowed = k_pos[None, :] <= q_pos[:, None]
    scores = jnp.where(allowed[None], scores, -jnp.inf)
    block_top = jnp.max(scores, axis=-1)
    weights = jnp.exp(scores - block_top[..., None])
    block_total = jnp.sum(weights, axis=-1)
    block_out = jnp.einsum(
        "hqk,khd->hqd", weights.astype(jnp.bfloat16), v_blk, preferred_element_type=jnp.float32
    ).astype(jnp.bfloat16)
    return (block_top, block_total, block_out)


def merge_terms(state, terms):
    top_now, total_now, acc_now = state
    block_top, block_total, block_out = terms
    top_new = jnp.maximum(top_now, block_top)
    keep_old = jnp.exp(top_now - top_new)
    keep_new = jnp.exp(block_top - top_new)
    return (
        top_new,
        total_now * keep_old + block_total * keep_new,
        acc_now * keep_old[..., None] + block_out.astype(jnp.float32) * keep_new[..., None],
    )


def local(
    inputs,
    norm_gain,
    w_conv_in,
    w_conv_gate,
    conv_kernel,
    ln_gain,
    w_query,
    w_key,
    w_value,
    cum_gate,
    w_conv_out,
    w_attn_out,
):
    rows_here = inputs.shape[0]
    conv_width = w_conv_in.shape[0]
    attn_width = w_query.shape[0]
    heads_here = cum_gate.shape[0]
    head_dim = attn_width // heads_here
    taps_count = conv_kernel.shape[0]
    w_all = jnp.concatenate([w_conv_in, w_conv_gate, w_query, w_key, w_value], axis=0)
    gain_all = norm_gain.astype(jnp.float32)
    contract_dims = (((1,), (1,)), ((), ()))
    piece_f = lax.all_gather(inputs, "tp", axis=1, tiled=True).astype(jnp.float32)
    scaled_piece = (piece_f * gain_all[None, :]).astype(jnp.bfloat16)
    raw_proj = lax.dot_general(
        scaled_piece, w_all, contract_dims, preferred_element_type=jnp.float32
    )
    squares = jnp.sum(piece_f * piece_f, axis=1)
    rms = lax.rsqrt(squares / D + 1e-06)[:, None]
    proj = raw_proj * rms
    conv_in = proj[:, :conv_width]
    conv_gate = proj[:, conv_width : 2 * conv_width]
    query = proj[:, 2 * conv_width : 2 * conv_width + attn_width].astype(jnp.bfloat16)
    key_rows = proj[:, 2 * conv_width + attn_width : 2 * conv_width + 2 * attn_width].astype(
        jnp.bfloat16
    )
    value = proj[:, 2 * conv_width + 2 * attn_width :].astype(jnp.bfloat16)
    glu = (conv_in * jax.nn.sigmoid(conv_gate)).astype(jnp.bfloat16)
    rim_rows = passed_along(glu[rows_here - (taps_count - 1) :], "sp", 1)
    extended = jnp.concatenate([rim_rows, glu], axis=0)
    kernel = conv_kernel.astype(jnp.float32)
    conv_sum = jnp.zeros((rows_here, conv_width), jnp.float32)
    for tap_idx in range(taps_count):
        conv_sum = (
            conv_sum
            + extended[tap_idx : tap_idx + rows_here].astype(jnp.float32) * kernel[tap_idx][None, :]
        )
    chan_first, chan_second = lax.psum(
        (jnp.sum(conv_sum, axis=1), jnp.sum(conv_sum * conv_sum, axis=1)), "tp"
    )
    chan_mean = (chan_first / CONV_CH)[:, None]
    chan_var = (chan_second / CONV_CH)[:, None] - chan_mean * chan_mean
    normed = (
        (conv_sum - chan_mean) * lax.rsqrt(chan_var + 1e-05) * ln_gain.astype(jnp.float32)[None, :]
    )
    conv_out = jax.nn.silu(normed).astype(jnp.bfloat16)
    q_heads = query.reshape(rows_here, heads_here, head_dim)
    cum_all = lax.all_gather(cum_gate.T, "sp", axis=0, tiled=True)
    own_first = lax.axis_index("sp") * rows_here
    start_state = (
        jnp.full((heads_here, rows_here), neg_large, jnp.float32),
        jnp.zeros((heads_here, rows_here), jnp.float32),
        jnp.zeros((heads_here, rows_here, head_dim), jnp.float32),
    )
    state = start_state
    k_piece = lax.all_gather(key_rows, "sp", axis=0, tiled=True)
    v_piece = lax.all_gather(value, "sp", axis=0, tiled=True)
    block_count = k_piece.shape[0] // rows_here
    k_split = k_piece.reshape(block_count, rows_here, heads_here, head_dim)
    v_split = v_piece.reshape(block_count, rows_here, heads_here, head_dim)

    def visit(carry, item):
        k_blk, v_blk, block_idx = item
        k_first = block_idx * rows_here
        k_cum = lax.dynamic_slice_in_dim(cum_all, k_first, rows_here, 0).T

        def take_block(inner):
            return merge_terms(
                inner, block_terms(q_heads, cum_gate, k_blk, v_blk, k_cum, own_first, k_first)
            )

        def skip_block(inner):
            return inner

        return (lax.cond(k_first <= own_first, take_block, skip_block, carry), None)

    state, unused = lax.scan(
        visit, state, (k_split, v_split, jnp.arange(block_count, dtype=jnp.int32))
    )
    top_all, total_all, acc_all = state
    attn_out = (
        (acc_all / total_all[..., None])
        .transpose(1, 0, 2)
        .reshape(rows_here, attn_width)
        .astype(jnp.bfloat16)
    )
    log_total = top_all + jnp.log(total_all)
    mixed = lax.psum_scatter(
        (
            jnp.dot(conv_out, w_conv_out, preferred_element_type=jnp.float32)
            + jnp.dot(attn_out, w_attn_out, preferred_element_type=jnp.float32)
        ).astype(jnp.bfloat16),
        "tp",
        scatter_dimension=0,
        tiled=True,
    )
    return (mixed, log_total)


AG_CHUNKS = 4
OUT_CHUNKS = 4
MESH = pl.DeviceIdType.MESH
NT = (((1,), (1,)), ((), ()))


def fused_kernel(
    n_sp,
    n_tp,
    x_hbm,
    gain_ref,
    wci_hbm,
    wcg_hbm,
    ck_ref,
    lng_ref,
    wq_hbm,
    wk_hbm,
    wv_hbm,
    cum_ref,
    wco_hbm,
    wao_hbm,
    out_ref,
    log_ref,
    xg,
    xs,
    wbuf,
    wco,
    wao,
    acc,
    ss,
    zsend,
    zrecv,
    q_s,
    k_s,
    v_s,
    v_t,
    out_loc,
    lse_loc,
    cum_col,
    cum_recv,
    ext,
    halo_src,
    halo,
    csum,
    st_send,
    st_recv,
    cpart,
    ret_send,
    ret_recv,
    att_s,
    lse_send,
    lse_recv,
    d_send,
    d_recv,
    x_send,
    x_recv,
    parts,
    wsem,
    owsem,
    xsem,
    ag_send,
    ag_recv,
    zs_sem,
    zr_sem,
    cs_sem,
    cr_sem,
    hs_sem,
    hr_sem,
    ss_sem,
    sr_sem,
    rs_sem,
    rr_sem,
    ls_sem,
    lr_sem,
    ds_sem,
    dr_sem,
    xs_sem,
    xr_sem,
):
    f32, bf16 = jnp.float32, jnp.bfloat16
    z = lax.axis_index("sp")
    me = lax.axis_index("tp")
    chip, core = me // 2, me % 2
    chips = n_tp // 2
    rows, width = x_hbm.shape
    conv_w = wci_hbm.shape[0]
    attn_w = wq_hbm.shape[0]
    heads = n_sp
    hd = attn_w // heads
    d_all = wci_hbm.shape[1]
    partner = chip * 2 + 1 - core

    def remote(src, dst, s, r, dev):
        return pltpu.make_async_remote_copy(
            src_ref=src, dst_ref=dst, send_sem=s, recv_sem=r, device_id=dev, device_id_type=MESH
        )

    def same_core(dist):
        return lax.rem(chip + dist, chips) * 2 + core

    def other_core(dist):
        return lax.rem(chip + dist, chips) * 2 + 1 - core

    def piece_owner(rel):
        return same_core(rel // 2) if rel % 2 == 0 else other_core(rel // 2)

    def piece_source(rel):
        back = chips - rel // 2
        return same_core(back) if rel % 2 == 0 else other_core(back)

    barrier = pltpu.get_barrier_semaphore()
    for rel in range(1, n_tp):
        pl.semaphore_signal(
            barrier, inc=1, device_id={"tp": piece_owner(rel)}, device_id_type=MESH
        )
    for dist in range(1, n_sp):
        pl.semaphore_signal(
            barrier, inc=1, device_id={"sp": lax.rem(z + dist, n_sp)}, device_id_type=MESH
        )

    own_copy = pltpu.make_async_copy(x_hbm, xg.at[0], xsem)
    own_copy.start()
    loads = []
    for h in range(heads):
        loads.append((wk_hbm.at[pl.ds(h * hd, hd)], wbuf.at[pl.ds(2 * h * hd, hd)]))
        loads.append((wv_hbm.at[pl.ds(h * hd, hd)], wbuf.at[pl.ds((2 * h + 1) * hd, hd)]))
    loads.append((wq_hbm, wbuf.at[pl.ds(2 * attn_w, attn_w)]))
    qkv_loads = len(loads)
    qkv_w = 3 * attn_w
    loads.append((wci_hbm, wbuf.at[pl.ds(qkv_w, conv_w)]))
    loads.append((wcg_hbm, wbuf.at[pl.ds(qkv_w + conv_w, conv_w)]))
    wcopies = [pltpu.make_async_copy(a, b, wsem.at[i]) for i, (a, b) in enumerate(loads)]
    wco_copy = pltpu.make_async_copy(wco_hbm, wco, owsem.at[0])
    wao_copy = pltpu.make_async_copy(wao_hbm, wao, owsem.at[1])
    for c in wcopies:
        c.start()
    wco_copy.start()
    wao_copy.start()

    pl.semaphore_wait(barrier, n_tp - 1 + n_sp - 1)

    rc = rows // AG_CHUNKS

    def ag_copy(rel, kind, c):
        r = pl.ds(c * rc, rc)
        if kind == "own":
            return remote(
                x_hbm.at[r], xg.at[rel, r], ag_send.at[rel, c], ag_recv.at[rel, c],
                {"tp": piece_owner(rel)},
            )
        return remote(
            xg.at[rel - 1, r], xg.at[rel, r], ag_send.at[rel, c], ag_recv.at[rel, c],
            {"tp": partner},
        )

    order = [AG_CHUNKS - 1] + list(range(AG_CHUNKS - 1))
    ag = {}
    for c in order:
        for dist in range(1, chips):
            ag[2 * dist, c] = ag_copy(2 * dist, "own", c)
            ag[2 * dist, c].start()
    for c in order:
        ag[1, c] = ag_copy(1, "own", c)
        ag[1, c].start()
    cums = []
    for dist in range(1, n_sp):
        cp = remote(
            cum_ref, cum_recv.at[z], cs_sem.at[dist], cr_sem.at[dist],
            {"sp": lax.rem(z + dist, n_sp)},
        )
        cp.start()
        cums.append(cp)
    cum_recv[z] = cum_ref[...]

    def prepare(rel, c0, n):
        r = pl.ds(c0, n)
        owner = piece_source(rel)
        raw = xg[rel, r].astype(f32)
        g = gain_ref[pl.ds(pl.multiple_of(owner * width, width), width)].astype(f32).reshape(1, width)
        xs[rel, r] = (raw * g).astype(bf16)
        return jnp.sum(raw * raw, axis=1, keepdims=True)

    def wcols(rel, first, n):
        owner = piece_source(rel)
        return wbuf[pl.ds(first, n), pl.ds(pl.multiple_of(owner * width, width), width)]

    own_copy.wait()
    ss[...] = prepare(0, 0, rows)
    for c in wcopies[:qkv_loads]:
        c.wait()
    acc[:, :qkv_w] = lax.dot_general(xs[0], wcols(0, 0, qkv_w), NT, preferred_element_type=f32)
    for c in wcopies[qkv_loads:]:
        c.wait()
    acc[:, qkv_w:] = lax.dot_general(
        xs[0], wcols(0, qkv_w, 2 * conv_w), NT, preferred_element_type=f32
    )
    for c in range(AG_CHUNKS):
        ag[1, c].wait_recv()
    ss[...] += prepare(1, 0, rows)
    acc[...] += lax.dot_general(
        xs[1], wcols(1, 0, qkv_w + 2 * conv_w), NT, preferred_element_type=f32
    )

    half = rc // 2
    spans = (pl.ds(0, rc), pl.ds(rc, half))

    def z_copy(dist, c, part):
        to = lax.rem(z + dist, n_sp)
        return remote(
            zsend.at[to, c, spans[part]],
            zrecv.at[z, c, spans[part]],
            zs_sem.at[dist, c, part],
            zr_sem.at[dist, c, part],
            {"sp": to},
        )

    def z_arrival(dist, c, part):
        src = lax.rem(z + n_sp - dist, n_sp)
        return remote(
            zsend.at[src, c, spans[part]],
            zrecv.at[src, c, spans[part]],
            zs_sem.at[dist, c, part],
            zr_sem.at[dist, c, part],
            {"sp": src},
        )

    def finish_chunk(c):
        r = pl.ds(c * rc, rc)
        total = acc[r, :qkv_w]
        sq = ss[r]
        for dist in range(1, chips):
            ag[2 * dist + 1, c].wait_recv()
            sq = sq + prepare(2 * dist + 1, c * rc, rc)
            total = total + lax.dot_general(
                xs[2 * dist + 1, r],
                wcols(2 * dist + 1, 0, qkv_w),
                NT,
                preferred_element_type=f32,
            )
        rms = lax.rsqrt(sq / d_all + 1e-06)
        ss[r] = rms
        total = total * rms
        for h in range(heads):
            zsend[h, c, :rc] = total[:, 2 * h * hd : 2 * (h + 1) * hd].astype(bf16)
            q_h = total[:, 2 * attn_w + h * hd : 2 * attn_w + (h + 1) * hd]
            zsend[h, c, rc:] = jnp.concatenate([q_h[:half], q_h[half:]], axis=1).astype(bf16)
        for dist in range(n_sp - 1, 0, -1):

            @pl.when(z < n_sp - 1)
            def _():
                z_copy(dist, c, 0).start()

            @pl.when(z > 0)
            def _():
                z_copy(dist, c, 1).start()

        zrecv[z, c] = zsend[z, c]

    rim = halo.shape[0]
    halo_copy = remote(
        halo_src, halo, hs_sem, hr_sem, {"sp": lax.rem(z + 1, n_sp)}
    )

    def gated(r):
        pre = acc[r, qkv_w:]
        for rel in range(2, n_tp):
            pre = pre + lax.dot_general(
                xs[rel, r], wcols(rel, qkv_w, 2 * conv_w), NT, preferred_element_type=f32
            )
        pre = pre * ss[r]
        return (pre[:, :conv_w] * jax.nn.sigmoid(pre[:, conv_w:])).astype(bf16)

    for k, c in enumerate(order):
        r = pl.ds(c * rc, rc)
        for dist in range(1, chips):
            ag[2 * dist, c].wait_recv()
            ag[2 * dist + 1, c] = ag_copy(2 * dist + 1, "relay", c)
            ag[2 * dist + 1, c].start()
        for dist in range(1, chips):
            ss[r] += prepare(2 * dist, c * rc, rc)
            acc[r, :qkv_w] += lax.dot_general(
                xs[2 * dist, r], wcols(2 * dist, 0, qkv_w), NT, preferred_element_type=f32
            )
        if k == 0:
            finish_chunk(c)
        elif k == 1:
            halo_src[...] = gated(pl.ds(rows - rim, rim))

            @pl.when(z < n_sp - 1)
            def _():
                halo_copy.start()

        else:
            finish_chunk(order[k - 1])
    finish_chunk(order[-1])

    glu = gated(pl.ds(0, rows))
    taps = ck_ref.shape[0]
    ext[rim:, :] = glu.astype(f32)
    blk = 64

    def conv_block(b, carry):
        first = pl.multiple_of(b * blk, blk)
        block = ext[pl.ds(first, blk + rim), :]
        tot = jnp.zeros((blk, conv_w), f32)
        for j in range(taps):
            off = rim - (taps - 1) + j
            tot = tot + block[off : off + blk] * ck_ref[j : j + 1, :].astype(f32)
        csum[pl.ds(first, blk), :] = tot
        return carry

    lax.fori_loop(1, rows // blk, conv_block, 0)
    for cp in cums:
        cp.wait_recv()
    for src in range(n_sp):
        cum_col[pl.ds(src * rows, rows)] = jnp.broadcast_to(
            cum_recv[src, pl.ds(z, 1)], (128, rows)
        ).T

    @pl.when(z == 0)
    def _():
        halo[...] = jnp.zeros_like(halo)

    @pl.when(z > 0)
    def _():
        halo_copy.wait_recv()

    ext[:rim, :] = halo[...].astype(f32)
    conv_block(0, 0)
    cs = csum[...]
    first = jnp.sum(cs, axis=1, keepdims=True)
    second = jnp.sum(cs * cs, axis=1, keepdims=True)
    lane = lax.broadcasted_iota(jnp.int32, (rows, 128), 1)
    both = jnp.where(lane == 0, first, second)
    st_send[...] = both.T[: st_send.shape[0]]
    stats = []
    for rel in range(1, n_tp):
        cp = remote(
            st_send, st_recv.at[rel - 1], ss_sem.at[rel], sr_sem.at[rel], {"tp": piece_owner(rel)}
        )
        cp.start()
        stats.append(cp)
    scale = hd ** (-0.5)
    low = lax.broadcasted_iota(jnp.int32, (rc, 2 * hd), 1) < hd
    wide_k = -(-rows // 128)
    allowed = lax.broadcasted_iota(jnp.int32, (rows, rows), 0) <= lax.broadcasted_iota(
        jnp.int32, (rows, rows), 1
    )

    def take_keys(tile, r0):
        kv = tile.astype(f32)
        k_s[pl.ds(r0, rc)] = kv[:, :hd].astype(bf16)
        v_s[pl.ds(r0, rc)] = jnp.where(low, pltpu.roll(kv, hd, 1), 1.0).astype(bf16)

    def take_queries(tile, r0):
        qt = tile.astype(f32) * scale
        q_s[pl.ds(r0, half)] = qt[:, :hd].astype(bf16)
        q_s[pl.ds(r0 + half, half)] = qt[:, hd:].astype(bf16)

    def attend(q, k, vt, cum_k, causal):
        sc = lax.dot_general(k, q, NT, preferred_element_type=f32) - cum_k
        if causal:
            sc = jnp.where(allowed, sc, -jnp.inf)
        top = jnp.max(sc, axis=0, keepdims=True)
        p = jnp.exp(sc - top).astype(bf16)
        both = jnp.dot(vt, p, preferred_element_type=f32)
        tot = both[hd : hd + 1]
        return both[:hd] / tot, top + jnp.log(tot)

    for h in range(heads):
        for c in range(AG_CHUNKS):
            take_keys(zsend[h, c, :rc], h * rows + c * rc)
            take_queries(zsend[h, c, rc:], h * rows + c * rc)
    v_t[...] = v_s[...].T
    for h in range(heads):
        own = pl.ds(h * rows, rows)
        own_cum = cum_ref[pl.ds(h, 1), :]
        col = jnp.broadcast_to(own_cum, (128, rows)).T
        out_loc[pl.ds(h * hd, hd), :], lse = attend(
            q_s[own], k_s[own], v_t[:, h * rows : (h + 1) * rows],
            jnp.concatenate([col] * wide_k, axis=1), True,
        )
        lse_loc[pl.ds(h, 1), :] = lse + own_cum
    for dist in range(1, n_sp):
        src = lax.rem(z + n_sp - dist, n_sp)
        for c in range(AG_CHUNKS):

            @pl.when(src < n_sp - 1)
            def _():
                z_arrival(dist, c, 0).wait_recv()

            @pl.when(src > 0)
            def _():
                z_arrival(dist, c, 1).wait_recv()

    for s in range(n_sp):
        for c in range(AG_CHUNKS):
            if s < n_sp - 1:
                take_keys(zrecv[s, c, :rc], s * rows + c * rc)
            if s > 0:
                take_queries(zrecv[s, c, rc:], s * rows + c * rc)
    far_keys = (n_sp - 1) * rows
    v_t[:, :far_keys] = v_s[:far_keys].T
    for i in [1 + k // 2 if k % 2 == 0 else n_sp - 1 - k // 2 for k in range(n_sp - 1)]:
        keys = i * rows
        o, lse = attend(
            q_s[pl.ds(i * rows, rows)], k_s[:keys], v_t[:, :keys],
            jnp.concatenate([cum_col[:keys]] * wide_k, axis=1), False,
        )
        ret_send[i] = o.astype(bf16)
        lse_send[i] = jnp.broadcast_to(lse + cum_recv[i, pl.ds(z, 1)], (8, rows))

        @pl.when(z != i)
        def _():
            remote(
                ret_send.at[i], ret_recv.at[z], rs_sem.at[i], rr_sem.at[z], {"sp": i}
            ).start()
            remote(
                lse_send.at[i], lse_recv.at[z], ls_sem.at[i], lr_sem.at[z], {"sp": i}
            ).start()

        @pl.when(z == i)
        def _():
            ret_recv[i] = ret_send[i]
            lse_recv[i] = lse_send[i]

    tot = st_send[...]
    for rel in range(1, n_tp):
        stats[rel - 1].wait_recv()
        tot = tot + st_recv[rel - 1]
    wide = jnp.concatenate([tot] * (128 // tot.shape[0]), axis=0).T
    mean = wide[:, 0:1] / CONV_CH
    var = wide[:, 1:2] / CONV_CH - mean * mean
    normed = (csum[...] - mean) * lax.rsqrt(var + 1e-05) * lng_ref[...].astype(f32).reshape(1, conv_w)
    conv_out = (normed / (1.0 + jnp.exp(-normed))).astype(bf16)
    wco_copy.wait()
    cpart[...] = jnp.dot(conv_out, wco[...], preferred_element_type=f32)

    for h in range(n_sp):

        @pl.when((z != h) & (z > 0))
        def _():
            remote(
                ret_send.at[h], ret_recv.at[h], rs_sem.at[h], rr_sem.at[h], {"sp": h}
            ).wait_recv()
            remote(
                lse_send.at[h], lse_recv.at[h], ls_sem.at[h], lr_sem.at[h], {"sp": h}
            ).wait_recv()

    @pl.when(z == 0)
    def _():
        log_ref[...] = lse_loc[...]

    @pl.when(z > 0)
    def _():
        for h in range(heads):
            r = pl.ds(h * hd, hd)
            near, far = lse_loc[pl.ds(h, 1), :], lse_recv[h, 0:1, :]
            top = jnp.maximum(near, far)
            w_near, w_far = jnp.exp(near - top), jnp.exp(far - top)
            tot = w_near + w_far
            out_loc[r, :] = (out_loc[r, :] * w_near + ret_recv[h].astype(f32) * w_far) / tot
            log_ref[pl.ds(h, 1), :] = top + jnp.log(tot)

    att_s[...] = out_loc[...].T.astype(bf16)
    wao_copy.wait()
    own_rows = rows // n_tp
    cw = d_all // OUT_CHUNKS
    mine = pl.ds(pl.multiple_of(core * own_rows, own_rows), own_rows)
    theirs = pl.ds(pl.multiple_of((1 - core) * own_rows, own_rows), own_rows)
    d2d, xc = {}, {}

    def exchange(dist):
        to_chip = lax.rem(chip + dist, chips)
        r = pl.ds(pl.multiple_of(to_chip * 2 * own_rows, 2 * own_rows), 2 * own_rows)
        for n in range(OUT_CHUNKS):
            cols = slice(n * cw, (n + 1) * cw)
            parts[dist, n] = cpart[r, cols] + jnp.dot(
                att_s[r, :], wao[:, cols], preferred_element_type=f32
            )
            d_send[dist, n] = parts[dist, n, theirs].astype(bf16)
            d2d[dist, n] = remote(
                d_send.at[dist, n],
                d_recv.at[dist, n],
                ds_sem.at[dist, n],
                dr_sem.at[dist, n],
                {"tp": partner},
            )
            d2d[dist, n].start()

    def forward(dist):
        for n in range(OUT_CHUNKS):
            d2d[dist, n].wait_recv()
            x_send[dist - 1, n] = (
                parts[dist, n, mine] + d_recv[dist, n].astype(f32)
            ).astype(bf16)
            xc[dist, n] = remote(
                x_send.at[dist - 1, n],
                x_recv.at[dist - 1, n],
                xs_sem.at[dist - 1, n],
                xr_sem.at[dist - 1, n],
                {"tp": same_core(dist)},
            )
            xc[dist, n].start()

    for dist in range(1, chips):
        exchange(dist)
    for dist in range(1, chips):
        forward(dist)
    exchange(0)
    for n in range(OUT_CHUNKS):
        d2d[0, n].wait_recv()
    for n in range(OUT_CHUNKS):
        tot = parts[0, n, mine] + d_recv[0, n].astype(f32)
        for dist in range(1, chips):
            xc[dist, n].wait_recv()
            tot = tot + x_recv[dist - 1, n].astype(f32)
        out_ref[:, n * cw : (n + 1) * cw] = tot.astype(bf16)

    for cp in list(ag.values()) + cums + stats + list(d2d.values()) + list(xc.values()):
        cp.wait_send()

    @pl.when(z < n_sp - 1)
    def _():
        halo_copy.wait_send()

    for dist in range(1, n_sp):
        for c in range(AG_CHUNKS):

            @pl.when(z < n_sp - 1)
            def _():
                z_copy(dist, c, 0).wait_send()

            @pl.when(z > 0)
            def _():
                z_copy(dist, c, 1).wait_send()

    for i in range(1, n_sp):

        @pl.when(z != i)
        def _():
            remote(
                ret_send.at[i], ret_recv.at[z], rs_sem.at[i], rr_sem.at[z], {"sp": i}
            ).wait_send()
            remote(
                lse_send.at[i], lse_recv.at[z], ls_sem.at[i], lr_sem.at[z], {"sp": i}
            ).wait_send()


def fused_local(
    n_sp,
    n_tp,
    inputs,
    norm_gain,
    w_conv_in,
    w_conv_gate,
    conv_kernel,
    ln_gain,
    w_query,
    w_key,
    w_value,
    cum_gate,
    w_conv_out,
    w_attn_out,
):
    f32, bf16 = jnp.float32, jnp.bfloat16
    rows, width = inputs.shape
    conv_w, d_all = w_conv_in.shape
    attn_w = w_query.shape[0]
    heads = cum_gate.shape[0]
    hd = attn_w // heads
    chips = n_tp // 2
    own_rows = rows // n_tp
    rc = rows // AG_CHUNKS
    rim = -(-(conv_kernel.shape[0] - 1) // 16) * 16
    cw = d_all // OUT_CHUNKS
    all_w = 3 * attn_w + 2 * conv_w
    dma = pltpu.SemaphoreType.DMA
    scratch = [
        pltpu.VMEM((n_tp, rows, width), bf16),
        pltpu.VMEM((n_tp, rows, width), bf16),
        pltpu.VMEM((all_w, d_all), bf16),
        pltpu.VMEM((conv_w, d_all), bf16),
        pltpu.VMEM((attn_w, d_all), bf16),
        pltpu.VMEM((rows, all_w), f32),
        pltpu.VMEM((rows, 1), f32),
        pltpu.VMEM((n_sp, AG_CHUNKS, rc + rc // 2, 2 * hd), bf16),
        pltpu.VMEM((n_sp, AG_CHUNKS, rc + rc // 2, 2 * hd), bf16),
        pltpu.VMEM((n_sp * rows, hd), bf16),
        pltpu.VMEM((n_sp * rows, hd), bf16),
        pltpu.VMEM((n_sp * rows, 2 * hd), bf16),
        pltpu.VMEM((2 * hd, n_sp * rows), bf16),
        pltpu.VMEM((attn_w, rows), f32),
        pltpu.VMEM((heads, rows), f32),
        pltpu.VMEM((n_sp * rows, 128), f32),
        pltpu.VMEM((n_sp, heads, rows), f32),
        pltpu.VMEM((rows + rim, conv_w), f32),
        pltpu.VMEM((rim, conv_w), bf16),
        pltpu.VMEM((rim, conv_w), bf16),
        pltpu.VMEM((rows, conv_w), f32),
        pltpu.VMEM((8, rows), f32),
        pltpu.VMEM((n_tp - 1, 8, rows), f32),
        pltpu.VMEM((rows, d_all), f32),
        pltpu.VMEM((n_sp, hd, rows), bf16),
        pltpu.VMEM((n_sp, hd, rows), bf16),
        pltpu.VMEM((rows, attn_w), bf16),
        pltpu.VMEM((n_sp, 8, rows), f32),
        pltpu.VMEM((n_sp, 8, rows), f32),
        pltpu.VMEM((chips, OUT_CHUNKS, own_rows, cw), bf16),
        pltpu.VMEM((chips, OUT_CHUNKS, own_rows, cw), bf16),
        pltpu.VMEM((chips - 1, OUT_CHUNKS, own_rows, cw), bf16),
        pltpu.VMEM((chips - 1, OUT_CHUNKS, own_rows, cw), bf16),
        pltpu.VMEM((chips, OUT_CHUNKS, 2 * own_rows, cw), f32),
        dma((2 * heads + 3,)),
        dma((2,)),
        dma,
        dma((n_tp, AG_CHUNKS)),
        dma((n_tp, AG_CHUNKS)),
        dma((n_sp, AG_CHUNKS, 2)),
        dma((n_sp, AG_CHUNKS, 2)),
        dma((n_sp,)),
        dma((n_sp,)),
        dma,
        dma,
        dma((n_tp,)),
        dma((n_tp,)),
        dma((n_sp,)),
        dma((n_sp,)),
        dma((n_sp,)),
        dma((n_sp,)),
        dma((chips, OUT_CHUNKS)),
        dma((chips, OUT_CHUNKS)),
        dma((chips - 1, OUT_CHUNKS)),
        dma((chips - 1, OUT_CHUNKS)),
    ]
    far = pl.BlockSpec(memory_space=pl.ANY)
    near = pl.BlockSpec(memory_space=pltpu.VMEM)
    mixed, log_total = pl.pallas_call(
        functools.partial(fused_kernel, n_sp, n_tp),
        out_shape=(
            pltpu.VMEM((own_rows, d_all), bf16),
            pltpu.VMEM((heads, rows), f32),
        ),
        in_specs=[far, near, far, far, near, near, far, far, far, near, far, far],
        out_specs=(near, near),
        scratch_shapes=scratch,
        compiler_params=pltpu.CompilerParams(
            collective_id=0, has_side_effects=True, vmem_limit_bytes=60 * 1024 * 1024
        ),
    )(
        inputs,
        norm_gain,
        w_conv_in,
        w_conv_gate,
        conv_kernel,
        ln_gain,
        w_query,
        w_key,
        w_value,
        cum_gate,
        w_conv_out,
        w_attn_out,
    )
    return (mixed, log_total)


def solution(mesh):
    in_specs = (
        P(("grp", "sp"), "tp"),
        P(),
        P("tp", None),
        P("tp", None),
        P(None, "tp"),
        P("tp"),
        P("tp", None),
        P("tp", None),
        P("tp", None),
        P("tp", ("grp", "sp")),
        P("tp", None),
        P("tp", None),
    )
    out_specs = (P(("grp", "sp", "tp"), None), P("tp", ("grp", "sp")))
    heads_here = HEADS // mesh.shape["tp"]
    fits = heads_here == mesh.shape["sp"] and mesh.shape["tp"] % 2 == 0
    body = functools.partial(fused_local, mesh.shape["sp"], mesh.shape["tp"]) if fits else local
    return jax.shard_map(body, mesh=mesh, in_specs=in_specs, out_specs=out_specs, check_vma=False)
```

profile of v0, /device:TPU:11, one launch (start us, length us, event | category | flops | bytes accessed | tf_op | source)
XLA Modules:
  0.0 35.5 jit_solution(15091003941161989857)
XLA Ops:
  0.6 33.5 %shard_map.131 = (bf16[64,2048]{1,0:T(8,128)(2,1)S(1)}, f32[4,256]{1,0:T(4,128)S(1)}) custom-call(bf16[256,512]{1,0:T(8,128)(2,1)} %x_hbm.1, bf16[2048]{0:T(1024)(128)(2,1)} %gain_ref.1, bf16[256,2048]{1,0:T(8,128)(2,1)} %wci_hbm.1, bf16[256,2048]{1,0:T(8,128)(2,1)} %wcg_hbm.1, bf16[31,256]{1,0:T(8,128)(2,1)} %ck_ref.1, bf16[256]{0:T(256)(128)(2,1)} %lng_ref.1, ...), custom_call_target="tpu_custom_call" | custom-call | tf_op jit(solution)/shard_map/pallas_call | solution.py:802
  34.2 0.7 %copy.16 = bf16[64,2048]{1,0:T(8,128)(2,1)} copy(bf16[64,2048]{1,0:T(8,128)(2,1)S(1)} %get-tuple-element.2) | data formatting | bytes 524288
  34.9 0.6 %copy.17 = f32[4,256]{1,0:T(4,128)} copy(f32[4,256]{1,0:T(4,128)S(1)} %get-tuple-element.3) | data formatting | bytes 8192
where the time goes:
time: 35.8 us; the launch traced here: 35.5 us
  Pallas kernels  33.5 us (94%)
  local copies, waits for them, and re-layouts  1.3 us (4%)
  between operations  0.64 us (2%)
    pallas_call x1, Pallas kernels, fused_local(): pl.pallas_call(functools.partial(fused_kernel, n_sp, n_tp), out_shape=(pl...  33.5 us
    unnamed x2, local copies, waits for them, and re-layouts  1.3 us

commit v1 on v0

v1 whole, which is shorter than its diff:
```python
import functools
import jax
import jax.numpy as jnp
from jax import lax
from jax.experimental import pallas as pl
from jax.experimental.pallas import tpu as pltpu
from jax.sharding import PartitionSpec as P

D = 2048
CONV_CH = 1024
HEADS = 16


neg_large = -1e30


def passed_along(block, axis, distance):
    devices = range(lax.axis_size(axis))
    route = [(i - distance, i) for i in devices if i - distance in devices]
    return lax.ppermute(block, axis, route)


def block_terms(q_blk, q_cum, k_blk, v_blk, k_cum, q_first, k_first):
    score_scale = q_blk.shape[2] ** (-0.5)
    scores = (
        jnp.einsum("qhd,khd->hqk", q_blk, k_blk, preferred_element_type=jnp.float32) * score_scale
    )
    scores = scores + q_cum[:, :, None] - k_cum[:, None, :]
    q_pos = q_first + jnp.arange(q_blk.shape[0], dtype=jnp.int32)
    k_pos = k_first + jnp.arange(k_blk.shape[0], dtype=jnp.int32)
    allowed = k_pos[None, :] <= q_pos[:, None]
    scores = jnp.where(allowed[None], scores, -jnp.inf)
    block_top = jnp.max(scores, axis=-1)
    weights = jnp.exp(scores - block_top[..., None])
    block_total = jnp.sum(weights, axis=-1)
    block_out = jnp.einsum(
        "hqk,khd->hqd", weights.astype(jnp.bfloat16), v_blk, preferred_element_type=jnp.float32
    ).astype(jnp.bfloat16)
    return (block_top, block_total, block_out)


def merge_terms(state, terms):
    top_now, total_now, acc_now = state
    block_top, block_total, block_out = terms
    top_new = jnp.maximum(top_now, block_top)
    keep_old = jnp.exp(top_now - top_new)
    keep_new = jnp.exp(block_top - top_new)
    return (
        top_new,
        total_now * keep_old + block_total * keep_new,
        acc_now * keep_old[..., None] + block_out.astype(jnp.float32) * keep_new[..., None],
    )


def local(
    inputs,
    norm_gain,
    w_conv_in,
    w_conv_gate,
    conv_kernel,
    ln_gain,
    w_query,
    w_key,
    w_value,
    cum_gate,
    w_conv_out,
    w_attn_out,
):
    rows_here = inputs.shape[0]
    conv_width = w_conv_in.shape[0]
    attn_width = w_query.shape[0]
    heads_here = cum_gate.shape[0]
    head_dim = attn_width // heads_here
    taps_count = conv_kernel.shape[0]
    w_all = jnp.concatenate([w_conv_in, w_conv_gate, w_query, w_key, w_value], axis=0)
    gain_all = norm_gain.astype(jnp.float32)
    contract_dims = (((1,), (1,)), ((), ()))
    piece_f = lax.all_gather(inputs, "tp", axis=1, tiled=True).astype(jnp.float32)
    scaled_piece = (piece_f * gain_all[None, :]).astype(jnp.bfloat16)
    raw_proj = lax.dot_general(
        scaled_piece, w_all, contract_dims, preferred_element_type=jnp.float32
    )
    squares = jnp.sum(piece_f * piece_f, axis=1)
    rms = lax.rsqrt(squares / D + 1e-06)[:, None]
    proj = raw_proj * rms
    conv_in = proj[:, :conv_width]
    conv_gate = proj[:, conv_width : 2 * conv_width]
    query = proj[:, 2 * conv_width : 2 * conv_width + attn_width].astype(jnp.bfloat16)
    key_rows = proj[:, 2 * conv_width + attn_width : 2 * conv_width + 2 * attn_width].astype(
        jnp.bfloat16
    )
    value = proj[:, 2 * conv_width + 2 * attn_width :].astype(jnp.bfloat16)
    glu = (conv_in * jax.nn.sigmoid(conv_gate)).astype(jnp.bfloat16)
    rim_rows = passed_along(glu[rows_here - (taps_count - 1) :], "sp", 1)
    extended = jnp.concatenate([rim_rows, glu], axis=0)
    kernel = conv_kernel.astype(jnp.float32)
    conv_sum = jnp.zeros((rows_here, conv_width), jnp.float32)
    for tap_idx in range(taps_count):
        conv_sum = (
            conv_sum
            + extended[tap_idx : tap_idx + rows_here].astype(jnp.float32) * kernel[tap_idx][None, :]
        )
    chan_first, chan_second = lax.psum(
        (jnp.sum(conv_sum, axis=1), jnp.sum(conv_sum * conv_sum, axis=1)), "tp"
    )
    chan_mean = (chan_first / CONV_CH)[:, None]
    chan_var = (chan_second / CONV_CH)[:, None] - chan_mean * chan_mean
    normed = (
        (conv_sum - chan_mean) * lax.rsqrt(chan_var + 1e-05) * ln_gain.astype(jnp.float32)[None, :]
    )
    conv_out = jax.nn.silu(normed).astype(jnp.bfloat16)
    q_heads = query.reshape(rows_here, heads_here, head_dim)
    cum_all = lax.all_gather(cum_gate.T, "sp", axis=0, tiled=True)
    own_first = lax.axis_index("sp") * rows_here
    start_state = (
        jnp.full((heads_here, rows_here), neg_large, jnp.float32),
        jnp.zeros((heads_here, rows_here), jnp.float32),
        jnp.zeros((heads_here, rows_here, head_dim), jnp.float32),
    )
    state = start_state
    k_piece = lax.all_gather(key_rows, "sp", axis=0, tiled=True)
    v_piece = lax.all_gather(value, "sp", axis=0, tiled=True)
    block_count = k_piece.shape[0] // rows_here
    k_split = k_piece.reshape(block_count, rows_here, heads_here, head_dim)
    v_split = v_piece.reshape(block_count, rows_here, heads_here, head_dim)

    def visit(carry, item):
        k_blk, v_blk, block_idx = item
        k_first = block_idx * rows_here
        k_cum = lax.dynamic_slice_in_dim(cum_all, k_first, rows_here, 0).T

        def take_block(inner):
            return merge_terms(
                inner, block_terms(q_heads, cum_gate, k_blk, v_blk, k_cum, own_first, k_first)
            )

        def skip_block(inner):
            return inner

        return (lax.cond(k_first <= own_first, take_block, skip_block, carry), None)

    state, unused = lax.scan(
        visit, state, (k_split, v_split, jnp.arange(block_count, dtype=jnp.int32))
    )
    top_all, total_all, acc_all = state
    attn_out = (
        (acc_all / total_all[..., None])
        .transpose(1, 0, 2)
        .reshape(rows_here, attn_width)
        .astype(jnp.bfloat16)
    )
    log_total = top_all + jnp.log(total_all)
    mixed = lax.psum_scatter(
        (
            jnp.dot(conv_out, w_conv_out, preferred_element_type=jnp.float32)
            + jnp.dot(attn_out, w_attn_out, preferred_element_type=jnp.float32)
        ).astype(jnp.bfloat16),
        "tp",
        scatter_dimension=0,
        tiled=True,
    )
    return (mixed, log_total)


AG_CHUNKS = 4
OUT_CHUNKS = 4
MESH = pl.DeviceIdType.MESH
NT = (((1,), (1,)), ((), ()))
KV, Q = 0, 1
CROSS, SAME, OTHER = 0, 1, 2
ROUTES = (
    ((3, KV, 3, CROSS), (2, KV, 2, CROSS), (3, KV, 1, OTHER), (1, KV, 1, SAME)),
    ((3, KV, 3, CROSS), (2, KV, 2, CROSS), (0, KV, 0, CROSS), (2, Q, 0, OTHER), (0, Q, 0, SAME)),
    ((0, Q, 0, CROSS), (1, Q, 1, CROSS), (3, Q, 3, CROSS), (0, KV, 3, OTHER), (3, KV, 3, SAME)),
    ((0, Q, 0, CROSS), (1, Q, 1, CROSS), (1, Q, 2, OTHER), (2, Q, 2, SAME)),
)


def fused_kernel(n_tp, names, *refs):
    f32, bf16 = jnp.float32, jnp.bfloat16
    R = dict(zip(names, refs, strict=True))
    x_hbm, wci_hbm, wcg_hbm = R["x_hbm"], R["wci_hbm"], R["wcg_hbm"]
    wq_hbm, wk_hbm, wv_hbm = R["wq_hbm"], R["wk_hbm"], R["wv_hbm"]
    out_ref, log_ref = R["out_ref"], R["log_ref"]
    xg, xs, wbuf, wco, wao, acc, ss = (
        R[n] for n in ("xg", "xs", "wbuf", "wco", "wao", "acc", "ss")
    )
    gain_ref, ck_ref, lng_ref, cum_ref = R["gain"], R["ck"], R["lng"], R["cum"]
    zsend, zrecv, zx = R["zsend"], R["zrecv"], R["zx"]
    q_s, k_s, v_s, v_t = R["q_s"], R["k_s"], R["v_s"], R["v_t"]
    out_loc, lse_loc, cum_col, cum_recv = R["out_loc"], R["lse_loc"], R["cum_col"], R["cum_recv"]
    ext, halo_src, halo, csum = R["ext"], R["halo_src"], R["halo"], R["csum"]
    st_send, st_recv, cpart = R["st_send"], R["st_recv"], R["cpart"]
    t2_o, t2_l, q_cum = R["t2_o"], R["t2_l"], R["q_cum"]
    ret_send, ret_recv, lse_send, lse_recv = (
        R["ret_send"], R["ret_recv"], R["lse_send"], R["lse_recv"],
    )
    d_send, d_recv, x_send, x_recv, parts = (
        R[n] for n in ("d_send", "d_recv", "x_send", "x_recv", "parts")
    )
    ld = R["ld"]
    n_sp = len(ROUTES)
    z = lax.axis_index("sp")
    me = lax.axis_index("tp")
    chip, core = me // 2, me % 2
    chips = n_tp // 2
    rows, width = x_hbm.shape
    conv_w = wci_hbm.shape[0]
    attn_w = wq_hbm.shape[0]
    heads = n_sp
    hd = attn_w // heads
    d_all = wci_hbm.shape[1]
    partner = chip * 2 + 1 - core
    upper = z // 2
    z_near = z + 1 - 2 * (z % 2)
    key_blk, query_blk = 2 * upper, 2 * upper + 1
    other_head = (1 - upper) * (z + 2) + upper * (3 - z)

    def remote(src, dst, s, r, dev):
        return pltpu.make_async_remote_copy(
            src_ref=src, dst_ref=dst, send_sem=s, recv_sem=r, device_id=dev, device_id_type=MESH
        )

    def settle(ref, sem):
        pltpu.make_async_copy(ref, ref, sem).wait()

    def same_core(dist):
        return lax.rem(chip + dist, chips) * 2 + core

    def other_core(dist):
        return lax.rem(chip + dist, chips) * 2 + 1 - core

    def piece_owner(rel):
        return same_core(rel // 2) if rel % 2 == 0 else other_core(rel // 2)

    def piece_source(rel):
        back = chips - rel // 2
        return same_core(back) if rel % 2 == 0 else other_core(back)

    barrier = pltpu.get_barrier_semaphore()
    for rel in range(1, n_tp):
        pl.semaphore_signal(
            barrier, inc=1, device_id={"tp": piece_owner(rel)}, device_id_type=MESH
        )
    for dist in range(1, n_sp):
        pl.semaphore_signal(
            barrier, inc=1, device_id={"sp": lax.rem(z + dist, n_sp)}, device_id_type=MESH
        )

    own_copy = pltpu.make_async_copy(x_hbm, xg.at[0], ld.at[0])
    own_copy.start()
    small = [
        pltpu.make_async_copy(R[n + "_hbm"], R[n], ld.at[5 + i])
        for i, n in enumerate(("gain", "ck", "lng", "cum"))
    ]
    for c in small:
        c.start()
    qkv_w = 3 * attn_w
    own_copy.wait()
    for h in range(heads):
        for i, w in enumerate((wk_hbm, wv_hbm)):
            pltpu.make_async_copy(
                w.at[pl.ds(h * hd, hd)], wbuf.at[pl.ds((2 * h + i) * hd, hd)], ld.at[1]
            ).start()
    pltpu.make_async_copy(wq_hbm, wbuf.at[pl.ds(2 * attn_w, attn_w)], ld.at[1]).start()
    pltpu.make_async_copy(wci_hbm, wbuf.at[pl.ds(qkv_w, conv_w)], ld.at[2]).start()
    pltpu.make_async_copy(wcg_hbm, wbuf.at[pl.ds(qkv_w + conv_w, conv_w)], ld.at[2]).start()
    wco_copy = pltpu.make_async_copy(R["wco_hbm"], wco, ld.at[3])
    wao_copy = pltpu.make_async_copy(R["wao_hbm"], wao, ld.at[4])
    wco_copy.start()
    wao_copy.start()

    pl.semaphore_wait(barrier, n_tp - 1 + n_sp - 1)

    rc = rows // AG_CHUNKS

    def ag_copy(rel, relay, c):
        r = pl.ds(c * rc, rc)
        src, to = (xg.at[rel - 1, r], partner) if relay else (xg.at[0, r], piece_owner(rel))
        return remote(src, xg.at[rel, r], R["ag_s"], R["ag_r"].at[rel - 2, c], {"tp": to})

    order = [AG_CHUNKS - 1] + list(range(AG_CHUNKS - 1))
    for c in order:
        for dist in range(1, chips):
            ag_copy(2 * dist, False, c).start()
    pair_copy = remote(xg.at[0], xg.at[1], R["ag_s"], R["ag_r1"], {"tp": partner})
    pair_copy.start()
    small[3].wait()
    for dist in range(1, n_sp):
        remote(
            cum_ref, cum_recv.at[z], R["cs"], R["cr"], {"sp": lax.rem(z + dist, n_sp)}
        ).start()
    cum_recv[z] = cum_ref[...]
    small[0].wait()

    def prepare(rel, c0, n):
        r = pl.ds(c0, n)
        owner = piece_source(rel)
        raw = xg[rel, r].astype(f32)
        g = gain_ref[pl.ds(pl.multiple_of(owner * width, width), width)].astype(f32).reshape(1, width)
        xs[rel, r] = (raw * g).astype(bf16)
        return jnp.sum(raw * raw, axis=1, keepdims=True)

    def wcols(rel, first, n):
        owner = piece_source(rel)
        return wbuf[pl.ds(first, n), pl.ds(pl.multiple_of(owner * width, width), width)]

    ss[...] = prepare(0, 0, rows)
    settle(wbuf.at[pl.ds(0, qkv_w)], ld.at[1])
    acc[:, :qkv_w] = lax.dot_general(xs[0], wcols(0, 0, qkv_w), NT, preferred_element_type=f32)
    settle(wbuf.at[pl.ds(qkv_w, 2 * conv_w)], ld.at[2])
    acc[:, qkv_w:] = lax.dot_general(
        xs[0], wcols(0, qkv_w, 2 * conv_w), NT, preferred_element_type=f32
    )
    pair_copy.wait_recv()
    ss[...] += prepare(1, 0, rows)
    acc[...] += lax.dot_general(
        xs[1], wcols(1, 0, qkv_w + 2 * conv_w), NT, preferred_element_type=f32
    )

    half = rc // 2
    spans = (pl.ds(0, rc), pl.ds(rc, half))

    def finish_chunk(c):
        r = pl.ds(c * rc, rc)
        total = acc[r, :qkv_w]
        sq = ss[r]
        for dist in range(1, chips):
            ag_copy(2 * dist + 1, True, c).wait_recv()
            sq = sq + prepare(2 * dist + 1, c * rc, rc)
            total = total + lax.dot_general(
                xs[2 * dist + 1, r],
                wcols(2 * dist + 1, 0, qkv_w),
                NT,
                preferred_element_type=f32,
            )
        rms = lax.rsqrt(sq / d_all + 1e-06)
        ss[r] = rms
        total = total * rms
        for h in range(heads):
            zsend[h, c, :rc] = total[:, 2 * h * hd : 2 * (h + 1) * hd].astype(bf16)
            q_h = total[:, 2 * attn_w + h * hd : 2 * attn_w + (h + 1) * hd]
            zsend[h, c, rc:] = jnp.concatenate([q_h[:half], q_h[half:]], axis=1).astype(bf16)
        for src, routes in enumerate(ROUTES):

            @pl.when(z == src)
            def _():
                for h, part, to, kind in routes:
                    dst = zx.at[c, spans[part]] if kind == OTHER else zrecv.at[src, c, spans[part]]
                    remote(
                        zsend.at[h, c, spans[part]], dst, R["zs"], R["zr"].at[kind], {"sp": to}
                    ).start()

        zrecv[z, c] = zsend[z, c]

        @pl.when(z % 2 == 0)
        def _():
            zx[c, :rc] = zsend[other_head, c, :rc]

        @pl.when(z % 2 == 1)
        def _():
            zx[c, rc:] = zsend[other_head, c, rc:]

    rim = halo.shape[0]
    halo_copy = remote(halo_src, halo, R["hs"], R["hr"], {"sp": lax.rem(z + 1, n_sp)})

    def gated(r):
        pre = acc[r, qkv_w:]
        for rel in range(2, n_tp):
            pre = pre + lax.dot_general(
                xs[rel, r], wcols(rel, qkv_w, 2 * conv_w), NT, preferred_element_type=f32
            )
        pre = pre * ss[r]
        return (pre[:, :conv_w] * jax.nn.sigmoid(pre[:, conv_w:])).astype(bf16)

    for k, c in enumerate(order):
        r = pl.ds(c * rc, rc)
        for dist in range(1, chips):
            ag_copy(2 * dist, False, c).wait_recv()
            ag_copy(2 * dist + 1, True, c).start()
        for dist in range(1, chips):
            ss[r] += prepare(2 * dist, c * rc, rc)
            acc[r, :qkv_w] += lax.dot_general(
                xs[2 * dist, r], wcols(2 * dist, 0, qkv_w), NT, preferred_element_type=f32
            )
        if k == 0:
            finish_chunk(c)
        elif k == 1:
            halo_src[...] = gated(pl.ds(rows - rim, rim))

            @pl.when(z < n_sp - 1)
            def _():
                halo_copy.start()

        else:
            finish_chunk(order[k - 1])
    finish_chunk(order[-1])

    glu = gated(pl.ds(0, rows))
    taps = ck_ref.shape[0]
    ext[rim:, :] = glu.astype(f32)
    blk = 64
    small[1].wait()
    small[2].wait()

    def conv_block(b, carry):
        first = pl.multiple_of(b * blk, blk)
        block = ext[pl.ds(first, blk + rim), :]
        tot = jnp.zeros((blk, conv_w), f32)
        for j in range(taps):
            off = rim - (taps - 1) + j
            tot = tot + block[off : off + blk] * ck_ref[j : j + 1, :].astype(f32)
        csum[pl.ds(first, blk), :] = tot
        return carry

    lax.fori_loop(1, rows // blk, conv_block, 0)
    settle(cum_recv.at[pl.ds(0, n_sp - 1)], R["cr"])
    for i, (src, h) in enumerate(((0, z), (1, z), (key_blk, z), (key_blk, other_head))):
        cum_col[pl.ds(i * rows, rows)] = jnp.broadcast_to(
            cum_recv[src, pl.ds(h, 1)], (128, rows)
        ).T

    @pl.when(z == 0)
    def _():
        halo[...] = jnp.zeros_like(halo)

    @pl.when(z > 0)
    def _():
        halo_copy.wait_recv()

    ext[:rim, :] = halo[...].astype(f32)
    conv_block(0, 0)
    cs = csum[...]
    first = jnp.sum(cs, axis=1, keepdims=True)
    second = jnp.sum(cs * cs, axis=1, keepdims=True)
    lane = lax.broadcasted_iota(jnp.int32, (rows, 128), 1)
    both = jnp.where(lane == 0, first, second)
    st_send[...] = both.T[: st_send.shape[0]]
    for rel in range(1, n_tp):
        remote(
            st_send, st_recv.at[rel - 1], R["st_s"], R["st_r"], {"tp": piece_owner(rel)}
        ).start()
    scale = hd ** (-0.5)
    low = lax.broadcasted_iota(jnp.int32, (rc, 2 * hd), 1) < hd
    wide_k = -(-rows // 128)
    allowed = lax.broadcasted_iota(jnp.int32, (rows, rows), 0) <= lax.broadcasted_iota(
        jnp.int32, (rows, rows), 1
    )

    def take_keys(tile, r0):
        kv = tile.astype(f32)
        k_s[pl.ds(r0, rc)] = kv[:, :hd].astype(bf16)
        v_s[pl.ds(r0, rc)] = jnp.where(low, pltpu.roll(kv, hd, 1), 1.0).astype(bf16)

    def take_queries(tile, r0):
        qt = tile.astype(f32) * scale
        q_s[pl.ds(r0, half)] = qt[:, :hd].astype(bf16)
        q_s[pl.ds(r0 + half, half)] = qt[:, hd:].astype(bf16)

    def attend(q, k, vt, cum_k, causal):
        sc = lax.dot_general(k, q, NT, preferred_element_type=f32) - cum_k
        if causal:
            sc = jnp.where(allowed, sc, -jnp.inf)
        top = jnp.max(sc, axis=0, keepdims=True)
        p = jnp.exp(sc - top).astype(bf16)
        both = jnp.dot(vt, p, preferred_element_type=f32)
        tot = both[hd : hd + 1]
        return both[:hd] / tot, top + jnp.log(tot)

    for h in range(heads):
        for c in range(AG_CHUNKS):
            take_keys(zsend[h, c, :rc], h * rows + c * rc)
            take_queries(zsend[h, c, rc:], h * rows + c * rc)
    v_t[...] = v_s[...].T
    for h in range(heads):
        own = pl.ds(h * rows, rows)
        own_cum = cum_ref[pl.ds(h, 1), :]
        col = jnp.broadcast_to(own_cum, (128, rows)).T
        out_loc[pl.ds(h * hd, hd), :], lse = attend(
            q_s[own], k_s[own], v_t[:, h * rows : (h + 1) * rows],
            jnp.concatenate([col] * wide_k, axis=1), True,
        )
        lse_loc[pl.ds(h, 1), :] = lse + own_cum

    qk_rows = half * 2 * hd * AG_CHUNKS // width

    def arrived(kind, units):
        for src, n in enumerate(units):

            @pl.when(z == src)
            def _():
                settle(xs.at[0, pl.ds(0, n * qk_rows)], R["zr"].at[kind])

    own_rows = rows // n_tp
    chip_rows = 2 * own_rows
    lanes = [
        pl.ds(pl.multiple_of(lax.rem(chip + 1 + i, chips) * chip_rows, chip_rows), chip_rows)
        for i in range(chips)
    ]

    def send_back(src_o, dst_o, src_l, dst_l, kind, to):
        remote(src_o, dst_o, R["rs"], R["rr"].at[kind], {"sp": to}).start()
        remote(src_l, dst_l, R["ls"], R["lr"].at[kind], {"sp": to}).start()

    arrived(OTHER, (1, 2, 1, 2))
    for c in range(AG_CHUNKS):
        take_keys(zx[c, :rc], c * rc)
        take_queries(zx[c, rc:], c * rc)
    v_t[:, :rows] = v_s[:rows].T
    o, lse = attend(
        q_s[:rows], k_s[:rows], v_t[:, :rows],
        jnp.concatenate([cum_col[3 * rows :]] * wide_k, axis=1), False,
    )
    lse = lse + cum_recv[query_blk, pl.ds(other_head, 1)]
    t2_o[...] = o
    t2_l[...] = lse
    slot = other_head + 4 * upper
    for i in range(chips):
        ret_send[3, i] = t2_o[:, lanes[i]].astype(bf16)
        lse_send[3, i] = t2_l[:, lanes[i]]

    @pl.when(z % 2 == 0)
    def _():
        send_back(
            ret_send.at[3], ret_recv.at[slot], lse_send.at[3], lse_recv.at[slot], 2, z + 1
        )

    @pl.when(z % 2 == 1)
    def _():
        ret_recv[slot] = ret_send[3]
        lse_recv[slot] = lse_send[3]

    arrived(SAME, (1, 2, 1, 2))
    for c in range(AG_CHUNKS):
        take_keys(zrecv[key_blk, c, :rc], c * rc)
        take_queries(zrecv[query_blk, c, rc:], c * rc)
    v_t[:, :rows] = v_s[:rows].T
    o, lse = attend(
        q_s[:rows], k_s[:rows], v_t[:, :rows],
        jnp.concatenate([cum_col[2 * rows : 3 * rows]] * wide_k, axis=1), False,
    )
    lse = lse + cum_recv[query_blk, pl.ds(z, 1)]
    t2_o[...] = o
    t2_l[...] = lse
    for i in range(chips):
        ret_send[2, i] = t2_o[:, lanes[i]].astype(bf16)
        lse_send[2, i] = t2_l[:, lanes[i]]

    @pl.when(z == 0)
    def _():
        send_back(ret_send.at[2], ret_recv.at[z], lse_send.at[2], lse_recv.at[z], 2, 1)

    @pl.when(z == 1)
    def _():
        ret_recv[z] = ret_send[2]
        lse_recv[z] = lse_send[2]

    settle(st_recv, R["st_r"])
    tot = st_send[...]
    for rel in range(1, n_tp):
        tot = tot + st_recv[rel - 1]
    wide = jnp.concatenate([tot] * (128 // tot.shape[0]), axis=0).T
    mean = wide[:, 0:1] / CONV_CH
    var = wide[:, 1:2] / CONV_CH - mean * mean
    normed = (csum[...] - mean) * lax.rsqrt(var + 1e-05) * lng_ref[...].astype(f32).reshape(1, conv_w)
    conv_out = (normed / (1.0 + jnp.exp(-normed))).astype(bf16)
    wco_copy.wait()
    cpart[...] = jnp.dot(conv_out, wco[...], preferred_element_type=f32)

    arrived(CROSS, (4, 2, 4, 5))
    for b in range(2):
        for c in range(AG_CHUNKS):
            take_keys(zrecv[b, c, :rc], b * rows + c * rc)
            take_queries(zrecv[2 + b, c, rc:], b * rows + c * rc)
    v_t[:, : 2 * rows] = v_s[: 2 * rows].T
    for b in range(2):
        q_cum[b : b + 1] = cum_recv[2 + b, pl.ds(z, 1)]
    for i in range(chips):
        q = jnp.concatenate(
            [
                q_s[pl.ds(pl.multiple_of(b * rows + lanes[i].start, chip_rows), chip_rows)]
                for b in range(2)
            ],
            axis=0,
        )
        o, lse = attend(
            q, k_s[: 2 * rows], v_t[:, : 2 * rows],
            jnp.concatenate([cum_col[: 2 * rows]] * (2 * chip_rows // 128), axis=1), False,
        )
        for b in range(2):
            o_b = o[:, b * chip_rows : (b + 1) * chip_rows]
            lse_b = lse[:, b * chip_rows : (b + 1) * chip_rows]
            lse_b = lse_b + q_cum[b : b + 1, lanes[i]]
            if b == 1:
                lse_n = jnp.where(upper == 1, t2_l[:, lanes[i]], neg_large)
                top = jnp.maximum(lse_b, lse_n)
                w_b, w_n = jnp.exp(lse_b - top), jnp.exp(lse_n - top)
                tot = w_b + w_n
                o_b = (o_b * w_b + t2_o[:, lanes[i]] * w_n) / tot
                lse_b = top + jnp.log(tot)
            ret_send[b, i] = o_b.astype(bf16)
            lse_send[b, i] = lse_b
        for b in range(1, -1, -1):

            @pl.when(z != 2 + b)
            def _():
                send_back(
                    ret_send.at[b, i], ret_recv.at[z, i],
                    lse_send.at[b, i], lse_recv.at[z, i], i, 2 + b,
                )

            @pl.when(z == 2 + b)
            def _():
                ret_recv[z, i] = ret_send[b, i]
                lse_recv[z, i] = lse_send[b, i]

    def merge(h, slot, i):
        r = pl.ds(h * hd, hd)
        near, far = lse_loc[pl.ds(h, 1), lanes[i]], lse_recv[slot, i]
        top = jnp.maximum(near, far)
        w_near, w_far = jnp.exp(near - top), jnp.exp(far - top)
        tot = w_near + w_far
        out_loc[r, lanes[i]] = (
            out_loc[r, lanes[i]] * w_near + ret_recv[slot, i].astype(f32) * w_far
        ) / tot
        lse_loc[pl.ds(h, 1), lanes[i]] = top + jnp.log(tot)

    @pl.when(z == 1)
    def _():
        settle(ret_recv.at[pl.ds(0, 2)], R["rr"].at[2])
        settle(lse_recv.at[pl.ds(0, 2)], R["lr"].at[2])
        for i in range(chips):
            for h in range(heads):
                merge(h, h, i)

    @pl.when(z == 3)
    def _():
        settle(ret_recv.at[pl.ds(0, 1)], R["rr"].at[2])
        settle(lse_recv.at[pl.ds(0, 1)], R["lr"].at[2])
        for i in range(chips):
            for h in range(2):
                merge(h, 4 + h, i)

    wao_copy.wait()
    cw = d_all // OUT_CHUNKS
    mine = pl.ds(pl.multiple_of(core * own_rows, own_rows), own_rows)
    theirs = pl.ds(pl.multiple_of((1 - core) * own_rows, own_rows), own_rows)

    def d_copy(dist, n):
        return remote(
            d_send.at[dist, n], d_recv.at[dist, n], R["ds"], R["dr"].at[dist, n], {"tp": partner}
        )

    def x_copy(n):
        return remote(x_send.at[n], x_recv.at[n], R["xs_s"], R["xr"].at[n], {"tp": same_core(1)})

    def exchange(dist):
        i = chips - 1 - dist

        @pl.when(z > 1)
        def _():
            settle(ret_recv.at[pl.ds(0, 3), i], R["rr"].at[i])
            settle(lse_recv.at[pl.ds(0, 3), i], R["lr"].at[i])
            for h in range(heads):
                merge(h, h, i)

        att = out_loc[:, lanes[i]].T.astype(bf16)
        for n in range(OUT_CHUNKS):
            cols = slice(n * cw, (n + 1) * cw)
            parts[dist, n] = cpart[lanes[i], cols] + jnp.dot(
                att, wao[:, cols], preferred_element_type=f32
            )
            d_send[dist, n] = parts[dist, n, theirs].astype(bf16)
            d_copy(dist, n).start()

    exchange(1)
    for n in range(OUT_CHUNKS):
        d_copy(1, n).wait_recv()
        x_send[n] = (parts[1, n, mine] + d_recv[1, n].astype(f32)).astype(bf16)
        x_copy(n).start()
    exchange(0)
    log_ref[...] = lse_loc[...]
    for n in range(OUT_CHUNKS):
        d_copy(0, n).wait_recv()
        tot = parts[0, n, mine] + d_recv[0, n].astype(f32)
        x_copy(n).wait_recv()
        tot = tot + x_recv[n].astype(f32)
        out_ref[:, n * cw : (n + 1) * cw] = tot.astype(bf16)

    settle(xg.at[pl.ds(1, n_tp - 1)], R["ag_s"])
    settle(cum_recv.at[pl.ds(0, n_sp - 1)], R["cs"])
    settle(st_recv, R["st_s"])
    settle(d_send, R["ds"])
    settle(x_send, R["xs_s"])

    @pl.when(z < n_sp - 1)
    def _():
        halo_copy.wait_send()

    sent = [sum(2 if r[1] == KV else 1 for r in routes) for routes in ROUTES]
    for src, (n, back) in enumerate(zip(sent, (4, 2, 2, 1), strict=True)):

        @pl.when(z == src)
        def _():
            settle(xs.at[0, pl.ds(0, n * qk_rows)], R["zs"])
            settle(ret_recv.at[pl.ds(0, back)], R["rs"])
            settle(lse_recv.at[pl.ds(0, back)], R["ls"])


def write_out(m_ref, l_ref, m_hbm, l_hbm, sem):
    a = pltpu.make_async_copy(m_ref, m_hbm, sem.at[0])
    b = pltpu.make_async_copy(l_ref, l_hbm, sem.at[1])
    a.start()
    b.start()
    a.wait()
    b.wait()


ARGS = (
    "x_hbm", "gain_hbm", "wci_hbm", "wcg_hbm", "ck_hbm", "lng_hbm",
    "wq_hbm", "wk_hbm", "wv_hbm", "cum_hbm", "wco_hbm", "wao_hbm",
)


def fused_local(n_tp, *args):
    f32, bf16 = jnp.float32, jnp.bfloat16
    inputs, norm_gain, w_conv_in, _, conv_kernel, ln_gain, w_query, _, _, cum_gate, _, _ = args
    n_sp = len(ROUTES)
    rows, width = inputs.shape
    conv_w, d_all = w_conv_in.shape
    attn_w = w_query.shape[0]
    heads = cum_gate.shape[0]
    hd = attn_w // heads
    chips = n_tp // 2
    own_rows = rows // n_tp
    rc = rows // AG_CHUNKS
    rim = -(-(conv_kernel.shape[0] - 1) // 16) * 16
    cw = d_all // OUT_CHUNKS
    all_w = 3 * attn_w + 2 * conv_w
    dma = pltpu.SemaphoreType.DMA
    vm = pltpu.VMEM
    scratch = {
        "xg": vm((n_tp, rows, width), bf16),
        "xs": vm((n_tp, rows, width), bf16),
        "wbuf": vm((all_w, d_all), bf16),
        "wco": vm((conv_w, d_all), bf16),
        "wao": vm((attn_w, d_all), bf16),
        "gain": vm(norm_gain.shape, bf16),
        "ck": vm(conv_kernel.shape, bf16),
        "lng": vm(ln_gain.shape, bf16),
        "cum": vm(cum_gate.shape, f32),
        "acc": vm((rows, all_w), f32),
        "ss": vm((rows, 1), f32),
        "zsend": vm((n_sp, AG_CHUNKS, rc + rc // 2, 2 * hd), bf16),
        "zrecv": vm((n_sp, AG_CHUNKS, rc + rc // 2, 2 * hd), bf16),
        "zx": vm((AG_CHUNKS, rc + rc // 2, 2 * hd), bf16),
        "q_s": vm((n_sp * rows, hd), bf16),
        "k_s": vm((n_sp * rows, hd), bf16),
        "v_s": vm((n_sp * rows, 2 * hd), bf16),
        "v_t": vm((2 * hd, n_sp * rows), bf16),
        "out_loc": vm((attn_w, rows), f32),
        "lse_loc": vm((heads, rows), f32),
        "cum_col": vm((4 * rows, 128), f32),
        "cum_recv": vm((n_sp, heads, rows), f32),
        "ext": vm((rows + rim, conv_w), f32),
        "halo_src": vm((rim, conv_w), bf16),
        "halo": vm((rim, conv_w), bf16),
        "csum": vm((rows, conv_w), f32),
        "st_send": vm((8, rows), f32),
        "st_recv": vm((n_tp - 1, 8, rows), f32),
        "cpart": vm((rows, d_all), f32),
        "t2_o": vm((hd, rows), f32),
        "t2_l": vm((1, rows), f32),
        "q_cum": vm((2, rows), f32),
        "ret_send": vm((4, chips, hd, 2 * own_rows), bf16),
        "ret_recv": vm((6, chips, hd, 2 * own_rows), bf16),
        "lse_send": vm((4, chips, 1, 2 * own_rows), f32),
        "lse_recv": vm((6, chips, 1, 2 * own_rows), f32),
        "d_send": vm((chips, OUT_CHUNKS, own_rows, cw), bf16),
        "d_recv": vm((chips, OUT_CHUNKS, own_rows, cw), bf16),
        "x_send": vm((OUT_CHUNKS, own_rows, cw), bf16),
        "x_recv": vm((OUT_CHUNKS, own_rows, cw), bf16),
        "parts": vm((chips, OUT_CHUNKS, 2 * own_rows, cw), f32),
        "ld": dma((9,)),
        "ag_s": dma,
        "ag_r1": dma,
        "ag_r": dma((n_tp - 2, AG_CHUNKS)),
        "zs": dma,
        "zr": dma((3,)),
        "cs": dma,
        "cr": dma,
        "hs": dma,
        "hr": dma,
        "st_s": dma,
        "st_r": dma,
        "rs": dma,
        "ls": dma,
        "rr": dma((3,)),
        "lr": dma((3,)),
        "ds": dma,
        "dr": dma((chips, OUT_CHUNKS)),
        "xs_s": dma,
        "xr": dma((OUT_CHUNKS,)),
    }
    far = pl.BlockSpec(memory_space=pl.ANY)
    near = pl.BlockSpec(memory_space=pltpu.VMEM)
    results = pl.pallas_call(
        functools.partial(fused_kernel, n_tp, ARGS + ("out_ref", "log_ref") + tuple(scratch)),
        out_shape=(
            pltpu.VMEM((own_rows, d_all), bf16),
            pltpu.VMEM((heads, rows), f32),
        ),
        in_specs=[far] * len(ARGS),
        out_specs=(near, near),
        scratch_shapes=list(scratch.values()),
        compiler_params=pltpu.CompilerParams(
            collective_id=0, has_side_effects=True, vmem_limit_bytes=60 * 1024 * 1024
        ),
    )(*args)
    return pl.pallas_call(
        write_out,
        out_shape=(
            jax.ShapeDtypeStruct((own_rows, d_all), bf16),
            jax.ShapeDtypeStruct((heads, rows), f32),
        ),
        in_specs=[near, near],
        out_specs=(far, far),
        scratch_shapes=[dma((2,))],
    )(*[pltpu.with_memory_space_constraint(r, pltpu.VMEM) for r in results])


def solution(mesh):
    in_specs = (
        P(("grp", "sp"), "tp"),
        P(),
        P("tp", None),
        P("tp", None),
        P(None, "tp"),
        P("tp"),
        P("tp", None),
        P("tp", None),
        P("tp", None),
        P("tp", ("grp", "sp")),
        P("tp", None),
        P("tp", None),
    )
    out_specs = (P(("grp", "sp", "tp"), None), P("tp", ("grp", "sp")))
    heads_here = HEADS // mesh.shape["tp"]
    fits = heads_here == mesh.shape["sp"] == len(ROUTES) and mesh.shape["tp"] == 4
    body = functools.partial(fused_local, mesh.shape["tp"]) if fits else local
    return jax.shard_map(body, mesh=mesh, in_specs=in_specs, out_specs=out_specs, check_vma=False)
```

time: 35.8 us -> 34 us (0.950)
  the two profiles are of different devices: /device:TPU:11 before, /device:TPU:21 now
where the time goes in v1:
time: 34 us; the launch traced here: 33.8 us
  Pallas kernels  33.2 us (98%)
  between operations  0.64 us (2%)
    pallas_call x1, Pallas kernels, fused_local(): pl.pallas_call(functools.partial(fused_kernel, n_tp, ARGS + ('out_ref', '...  32.5 us
    pallas_call x1, Pallas kernels, fused_local(): pl.pallas_call(write_out, out_shape=(jax.ShapeDtypeStruct((own_rows, d_al...  0.72 us

profile of v1, /device:TPU:21, one launch (start us, length us, event | category | flops | bytes accessed | tf_op | source)
XLA Modules:
  0.0 33.8 jit_solution(2205153872103716979)
XLA Ops:
  0.6 32.5 %shard_map.131 = (bf16[64,2048]{1,0:T(8,128)(2,1)S(1)}, f32[4,256]{1,0:T(4,128)S(1)}) custom-call(bf16[256,512]{1,0:T(8,128)(2,1)} %refs_0_.1, bf16[2048]{0:T(1024)(128)(2,1)} %refs_1_.1, bf16[256,2048]{1,0:T(8,128)(2,1)} %refs_2_.1, bf16[256,2048]{1,0:T(8,128)(2,1)} %refs_3_.1, bf16[31,256]{1,0:T(8,128)(2,1)} %refs_4_.1, bf16[256]{0:T(256)(128)(2,1)} %refs_5_.1, ...), custom_call_target="tpu_custom_call" | custom-call | tf_op jit(solution)/shard_map/pallas_call | solution.py:807
  33.1 0.7 %shard_map.132 = (bf16[64,2048]{1,0:T(8,128)(2,1)}, f32[4,256]{1,0:T(4,128)}) custom-call(bf16[64,2048]{1,0:T(8,128)(2,1)S(1)} %get-tuple-element.4.m_ref, f32[4,256]{1,0:T(4,128)S(1)} %get-tuple-element.5.l_ref), custom_call_target="tpu_custom_call" | custom-call | tf_op jit(solution)/shard_map/pallas_call | solution.py:820

commit v2 on v1

--- a/solution.py
+++ b/solution.py
@@ -169,11 +169,20 @@
 KV, Q = 0, 1
 CROSS, SAME, OTHER = 0, 1, 2
 ROUTES = (
-    ((3, KV, 3, CROSS), (2, KV, 2, CROSS), (3, KV, 1, OTHER), (1, KV, 1, SAME)),
-    ((3, KV, 3, CROSS), (2, KV, 2, CROSS), (0, KV, 0, CROSS), (2, Q, 0, OTHER), (0, Q, 0, SAME)),
-    ((0, Q, 0, CROSS), (1, Q, 1, CROSS), (3, Q, 3, CROSS), (0, KV, 3, OTHER), (3, KV, 3, SAME)),
-    ((0, Q, 0, CROSS), (1, Q, 1, CROSS), (1, Q, 2, OTHER), (2, Q, 2, SAME)),
+    ((3, KV, 3, CROSS), (2, KV, 2, CROSS), (1, KV, 1, SAME), (3, KV, 1, OTHER)),
+    ((3, KV, 3, CROSS), (2, KV, 2, CROSS), (0, KV, 0, CROSS), (0, Q, 0, SAME), (2, Q, 0, OTHER)),
+    ((0, Q, 0, CROSS), (1, Q, 1, CROSS), (3, Q, 3, CROSS), (3, KV, 3, SAME), (0, KV, 3, OTHER)),
+    ((0, Q, 0, CROSS), (1, Q, 1, CROSS), (2, Q, 2, SAME), (1, Q, 2, OTHER)),
 )
+OTHER_HEAD = (2, 3, 1, 0)
+TASKS = (
+    ((CROSS, 0), (SAME, 0), (OTHER, 0)),
+    ((CROSS, 0), (SAME, 0), (OTHER, 0), (CROSS, 1)),
+    ((SAME, 0), (OTHER, 0), (CROSS, 0), (CROSS, 1)),
+    ((SAME, 0), (OTHER, 0), (CROSS, 0), (CROSS, 1)),
+)
+LATE_TASKS = (((CROSS, 1),), (), (), ())
+ROW_GROUPS = ((3,), (0,), (1, 2))
 
 
 def fused_kernel(n_tp, names, *refs):
@@ -191,7 +200,7 @@
     out_loc, lse_loc, cum_col, cum_recv = R["out_loc"], R["lse_loc"], R["cum_col"], R["cum_recv"]
     ext, halo_src, halo, csum = R["ext"], R["halo_src"], R["halo"], R["csum"]
     st_send, st_recv, cpart = R["st_send"], R["st_recv"], R["cpart"]
-    t2_o, t2_l, q_cum = R["t2_o"], R["t2_l"], R["q_cum"]
+    t2_o, t2_l, s_o, s_l = R["t2_o"], R["t2_l"], R["s_o"], R["s_l"]
     ret_send, ret_recv, lse_send, lse_recv = (
         R["ret_send"], R["ret_recv"], R["lse_send"], R["lse_recv"],
     )
@@ -211,10 +220,6 @@
     hd = attn_w // heads
     d_all = wci_hbm.shape[1]
     partner = chip * 2 + 1 - core
-    upper = z // 2
-    z_near = z + 1 - 2 * (z % 2)
-    key_blk, query_blk = 2 * upper, 2 * upper + 1
-    other_head = (1 - upper) * (z + 2) + upper * (3 - z)
 
     def remote(src, dst, s, r, dev):
         return pltpu.make_async_remote_copy(
@@ -321,13 +326,14 @@
     half = rc // 2
     spans = (pl.ds(0, rc), pl.ds(rc, half))
 
-    def finish_chunk(c):
-        r = pl.ds(c * rc, rc)
+    def finish(group):
+        r = pl.ds(group[0] * rc, len(group) * rc)
         total = acc[r, :qkv_w]
         sq = ss[r]
         for dist in range(1, chips):
-            ag_copy(2 * dist + 1, True, c).wait_recv()
-            sq = sq + prepare(2 * dist + 1, c * rc, rc)
+            for c in group:
+                ag_copy(2 * dist + 1, True, c).wait_recv()
+            sq = sq + prepare(2 * dist + 1, group[0] * rc, len(group) * rc)
             total = total + lax.dot_general(
                 xs[2 * dist + 1, r],
                 wcols(2 * dist + 1, 0, qkv_w),
@@ -337,6 +343,10 @@
         rms = lax.rsqrt(sq / d_all + 1e-06)
         ss[r] = rms
         total = total * rms
+        for i, c in enumerate(group):
+            push(c, total[i * rc : (i + 1) * rc])
+
+    def push(c, total):
         for h in range(heads):
             zsend[h, c, :rc] = total[:, 2 * h * hd : 2 * (h + 1) * hd].astype(bf16)
             q_h = total[:, 2 * attn_w + h * hd : 2 * attn_w + (h + 1) * hd]
@@ -350,16 +360,6 @@
                     remote(
                         zsend.at[h, c, spans[part]], dst, R["zs"], R["zr"].at[kind], {"sp": to}
                     ).start()
-
-        zrecv[z, c] = zsend[z, c]
-
-        @pl.when(z % 2 == 0)
-        def _():
-            zx[c, :rc] = zsend[other_head, c, :rc]
-
-        @pl.when(z % 2 == 1)
-        def _():
-            zx[c, rc:] = zsend[other_head, c, rc:]
 
     rim = halo.shape[0]
     halo_copy = remote(halo_src, halo, R["hs"], R["hr"], {"sp": lax.rem(z + 1, n_sp)})
@@ -373,73 +373,38 @@
         pre = pre * ss[r]
         return (pre[:, :conv_w] * jax.nn.sigmoid(pre[:, conv_w:])).astype(bf16)
 
-    for k, c in enumerate(order):
-        r = pl.ds(c * rc, rc)
+    def relay(c):
         for dist in range(1, chips):
             ag_copy(2 * dist, False, c).wait_recv()
             ag_copy(2 * dist + 1, True, c).start()
+
+    def add_crossed(group):
+        r = pl.ds(group[0] * rc, len(group) * rc)
         for dist in range(1, chips):
-            ss[r] += prepare(2 * dist, c * rc, rc)
+            ss[r] += prepare(2 * dist, group[0] * rc, len(group) * rc)
             acc[r, :qkv_w] += lax.dot_general(
                 xs[2 * dist, r], wcols(2 * dist, 0, qkv_w), NT, preferred_element_type=f32
             )
-        if k == 0:
-            finish_chunk(c)
-        elif k == 1:
-            halo_src[...] = gated(pl.ds(rows - rim, rim))
-
-            @pl.when(z < n_sp - 1)
-            def _():
-                halo_copy.start()
-
-        else:
-            finish_chunk(order[k - 1])
-    finish_chunk(order[-1])
+
+    relay(3)
+    add_crossed(ROW_GROUPS[0])
+    finish(ROW_GROUPS[0])
+    relay(0)
+    add_crossed(ROW_GROUPS[1])
+    halo_src[...] = gated(pl.ds(rows - rim, rim))
+
+    @pl.when(z < n_sp - 1)
+    def _():
+        halo_copy.start()
+
+    relay(1)
+    finish(ROW_GROUPS[1])
+    relay(2)
+    add_crossed(ROW_GROUPS[2])
+    finish(ROW_GROUPS[2])
 
     glu = gated(pl.ds(0, rows))
-    taps = ck_ref.shape[0]
     ext[rim:, :] = glu.astype(f32)
-    blk = 64
-    small[1].wait()
-    small[2].wait()
-
-    def conv_block(b, carry):
-        first = pl.multiple_of(b * blk, blk)
-        block = ext[pl.ds(first, blk + rim), :]
-        tot = jnp.zeros((blk, conv_w), f32)
-        for j in range(taps):
-            off = rim - (taps - 1) + j
-            tot = tot + block[off : off + blk] * ck_ref[j : j + 1, :].astype(f32)
-        csum[pl.ds(first, blk), :] = tot
-        return carry
-
-    lax.fori_loop(1, rows // blk, conv_block, 0)
-    settle(cum_recv.at[pl.ds(0, n_sp - 1)], R["cr"])
-    for i, (src, h) in enumerate(((0, z), (1, z), (key_blk, z), (key_blk, other_head))):
-        cum_col[pl.ds(i * rows, rows)] = jnp.broadcast_to(
-            cum_recv[src, pl.ds(h, 1)], (128, rows)
-        ).T
-
-    @pl.when(z == 0)
-    def _():
-        halo[...] = jnp.zeros_like(halo)
-
-    @pl.when(z > 0)
-    def _():
-        halo_copy.wait_recv()
-
-    ext[:rim, :] = halo[...].astype(f32)
-    conv_block(0, 0)
-    cs = csum[...]
-    first = jnp.sum(cs, axis=1, keepdims=True)
-    second = jnp.sum(cs * cs, axis=1, keepdims=True)
-    lane = lax.broadcasted_iota(jnp.int32, (rows, 128), 1)
-    both = jnp.where(lane == 0, first, second)
-    st_send[...] = both.T[: st_send.shape[0]]
-    for rel in range(1, n_tp):
-        remote(
-            st_send, st_recv.at[rel - 1], R["st_s"], R["st_r"], {"tp": piece_owner(rel)}
-        ).start()
     scale = hd ** (-0.5)
     low = lax.broadcasted_iota(jnp.int32, (rc, 2 * hd), 1) < hd
     wide_k = -(-rows // 128)
@@ -484,12 +449,49 @@
 
     qk_rows = half * 2 * hd * AG_CHUNKS // width
 
-    def arrived(kind, units):
-        for src, n in enumerate(units):
-
-            @pl.when(z == src)
-            def _():
-                settle(xs.at[0, pl.ds(0, n * qk_rows)], R["zr"].at[kind])
+    taps = ck_ref.shape[0]
+    blk = 64
+    small[1].wait()
+    small[2].wait()
+
+    def conv_block(b, carry):
+        first = pl.multiple_of(b * blk, blk)
+        block = ext[pl.ds(first, blk + rim), :]
+        tot = jnp.zeros((blk, conv_w), f32)
+        for j in range(taps):
+            off = rim - (taps - 1) + j
+            tot = tot + block[off : off + blk] * ck_ref[j : j + 1, :].astype(f32)
+        csum[pl.ds(first, blk), :] = tot
+        return carry
+
+    lax.fori_loop(1, rows // blk, conv_block, 0)
+
+    @pl.when(z == 0)
+    def _():
+        halo[...] = jnp.zeros_like(halo)
+
+    @pl.when(z > 0)
+    def _():
+        halo_copy.wait_recv()
+
+    ext[:rim, :] = halo[...].astype(f32)
+    conv_block(0, 0)
+    cs = csum[...]
+    first = jnp.sum(cs, axis=1, keepdims=True)
+    second = jnp.sum(cs * cs, axis=1, keepdims=True)
+    lane = lax.broadcasted_iota(jnp.int32, (rows, 128), 1)
+    both = jnp.where(lane == 0, first, second)
+    st_send[...] = both.T[: st_send.shape[0]]
+    for rel in range(1, n_tp):
+        remote(
+            st_send, st_recv.at[rel - 1], R["st_s"], R["st_r"], {"tp": piece_owner(rel)}
+        ).start()
+    settle(cum_recv.at[pl.ds(0, n_sp - 1)], R["cr"])
+
+    received = [[0] * 3 for _ in ROUTES]
+    for routes in ROUTES:
+        for _, part, to, kind in routes:
+            received[to][kind] += 2 if part == KV else 1
 
     own_rows = rows // n_tp
     chip_rows = 2 * own_rows
@@ -502,58 +504,103 @@
         remote(src_o, dst_o, R["rs"], R["rr"].at[kind], {"sp": to}).start()
         remote(src_l, dst_l, R["ls"], R["lr"].at[kind], {"sp": to}).start()
 
-    arrived(OTHER, (1, 2, 1, 2))
-    for c in range(AG_CHUNKS):
-        take_keys(zx[c, :rc], c * rc)
-        take_queries(zx[c, rc:], c * rc)
-    v_t[:, :rows] = v_s[:rows].T
-    o, lse = attend(
-        q_s[:rows], k_s[:rows], v_t[:, :rows],
-        jnp.concatenate([cum_col[3 * rows :]] * wide_k, axis=1), False,
-    )
-    lse = lse + cum_recv[query_blk, pl.ds(other_head, 1)]
-    t2_o[...] = o
-    t2_l[...] = lse
-    slot = other_head + 4 * upper
-    for i in range(chips):
-        ret_send[3, i] = t2_o[:, lanes[i]].astype(bf16)
-        lse_send[3, i] = t2_l[:, lanes[i]]
-
-    @pl.when(z % 2 == 0)
-    def _():
-        send_back(
-            ret_send.at[3], ret_recv.at[slot], lse_send.at[3], lse_recv.at[slot], 2, z + 1
-        )
-
-    @pl.when(z % 2 == 1)
-    def _():
-        ret_recv[slot] = ret_send[3]
-        lse_recv[slot] = lse_send[3]
-
-    arrived(SAME, (1, 2, 1, 2))
-    for c in range(AG_CHUNKS):
-        take_keys(zrecv[key_blk, c, :rc], c * rc)
-        take_queries(zrecv[query_blk, c, rc:], c * rc)
-    v_t[:, :rows] = v_s[:rows].T
-    o, lse = attend(
-        q_s[:rows], k_s[:rows], v_t[:, :rows],
-        jnp.concatenate([cum_col[2 * rows : 3 * rows]] * wide_k, axis=1), False,
-    )
-    lse = lse + cum_recv[query_blk, pl.ds(z, 1)]
-    t2_o[...] = o
-    t2_l[...] = lse
-    for i in range(chips):
-        ret_send[2, i] = t2_o[:, lanes[i]].astype(bf16)
-        lse_send[2, i] = t2_l[:, lanes[i]]
-
-    @pl.when(z == 0)
-    def _():
-        send_back(ret_send.at[2], ret_recv.at[z], lse_send.at[2], lse_recv.at[z], 2, 1)
-
-    @pl.when(z == 1)
-    def _():
-        ret_recv[z] = ret_send[2]
-        lse_recv[z] = lse_send[2]
+    def tile(zz, src, h, c):
+        if src == zz:
+            return zsend.at[h, c]
+        return zrecv.at[src, c] if h == zz else zx.at[c]
+
+    def far_terms(zz, h, r0, key_blks, query_blks):
+        for i, b in enumerate(key_blks):
+            for c in range(AG_CHUNKS):
+                take_keys(tile(zz, b, h, c)[:rc], r0 + i * rows + c * rc)
+            cum_col[pl.ds(r0 + i * rows, rows)] = jnp.broadcast_to(
+                cum_recv[b, h : h + 1], (128, rows)
+            ).T
+        for i, b in enumerate(query_blks):
+            for c in range(AG_CHUNKS):
+                take_queries(tile(zz, b, h, c)[rc:], r0 + i * rows + c * rc)
+        keys = slice(r0, r0 + len(key_blks) * rows)
+        v_t[:, keys] = v_s[keys].T
+
+    def far_attend(q, r0, n_k):
+        keys = slice(r0, r0 + n_k)
+        cum_k = jnp.concatenate([cum_col[keys]] * wide_k, axis=1)
+        return attend(q, k_s[keys], v_t[:, keys], cum_k, False)
+
+    def far_part(zz, tasks, seen):
+        upper = zz // 2
+        key_blk, query_blk = 2 * upper, 2 * upper + 1
+        later = []
+
+        def arrived(*kinds):
+            for kind in kinds:
+                if kind not in seen:
+                    seen.add(kind)
+                    n = received[zz][kind] * qk_rows
+                    settle(xs.at[0, pl.ds(0, n)], R["zr"].at[kind])
+
+        def hand_over(send, slot, i, to, o, lse):
+            if to == zz:
+                ret_recv[slot, i] = o.astype(bf16)
+                lse_recv[slot, i] = lse
+                return
+            ret_send[send, i] = o.astype(bf16)
+            lse_send[send, i] = lse
+            args = (
+                ret_send.at[send, i], ret_recv.at[slot, i],
+                lse_send.at[send, i], lse_recv.at[slot, i], i, to,
+            )
+            if i == 0:
+                send_back(*args)
+            else:
+                later.append(args)
+
+        for kind, i in tasks:
+            arrived(*((SAME, CROSS) if kind == CROSS else (kind,)))
+            if kind == CROSS:
+                if i == 0:
+                    far_terms(zz, zz, 0, (0, 1), (2, 3))
+                q = jnp.concatenate(
+                    [
+                        q_s[pl.ds(pl.multiple_of(b * rows + lanes[i].start, chip_rows), chip_rows)]
+                        for b in range(2)
+                    ],
+                    axis=0,
+                )
+                o, lse = far_attend(q, 0, 2 * rows)
+                for b in range(1, -1, -1):
+                    o_b = o[:, b * chip_rows : (b + 1) * chip_rows]
+                    lse_b = lse[:, b * chip_rows : (b + 1) * chip_rows]
+                    lse_b = lse_b + cum_recv[2 + b, zz : zz + 1, lanes[i]]
+                    if b == 1 and upper:
+                        lse_n = s_l[:, lanes[i]]
+                        top = jnp.maximum(lse_b, lse_n)
+                        w_b, w_n = jnp.exp(lse_b - top), jnp.exp(lse_n - top)
+                        tot = w_b + w_n
+                        o_b = (o_b * w_b + s_o[:, lanes[i]] * w_n) / tot
+                        lse_b = top + jnp.log(tot)
+                    hand_over(b, zz, i, 2 + b, o_b, lse_b)
+                continue
+            h, r0 = (zz, 2 * rows) if kind == SAME else (OTHER_HEAD[zz], 3 * rows)
+            far_terms(zz, h, r0, (key_blk,), (query_blk,))
+            o, lse = far_attend(q_s[r0 : r0 + rows], r0, rows)
+            o_ref, l_ref = (s_o, s_l) if kind == SAME else (t2_o, t2_l)
+            o_ref[...] = o
+            l_ref[...] = lse + cum_recv[query_blk, h : h + 1]
+            if kind == OTHER or not upper:
+                for n in range(chips):
+                    hand_over(
+                        kind + 1, h + 4 * upper if kind == OTHER else h, n, query_blk,
+                        o_ref[:, lanes[n]], l_ref[:, lanes[n]],
+                    )
+        for args in later:
+            send_back(*args)
+
+    for zz in range(n_sp):
+
+        @pl.when(z == zz)
+        def _():
+            far_part(zz, TASKS[zz], set())
 
     settle(st_recv, R["st_r"])
     tot = st_send[...]
@@ -567,53 +614,6 @@
     wco_copy.wait()
     cpart[...] = jnp.dot(conv_out, wco[...], preferred_element_type=f32)
 
-    arrived(CROSS, (4, 2, 4, 5))
-    for b in range(2):
-        for c in range(AG_CHUNKS):
-            take_keys(zrecv[b, c, :rc], b * rows + c * rc)
-            take_queries(zrecv[2 + b, c, rc:], b * rows + c * rc)
-    v_t[:, : 2 * rows] = v_s[: 2 * rows].T
-    for b in range(2):
-        q_cum[b : b + 1] = cum_recv[2 + b, pl.ds(z, 1)]
-    for i in range(chips):
-        q = jnp.concatenate(
-            [
-                q_s[pl.ds(pl.multiple_of(b * rows + lanes[i].start, chip_rows), chip_rows)]
-                for b in range(2)
-            ],
-            axis=0,
-        )
-        o, lse = attend(
-            q, k_s[: 2 * rows], v_t[:, : 2 * rows],
-            jnp.concatenate([cum_col[: 2 * rows]] * (2 * chip_rows // 128), axis=1), False,
-        )
-        for b in range(2):
-            o_b = o[:, b * chip_rows : (b + 1) * chip_rows]
-            lse_b = lse[:, b * chip_rows : (b + 1) * chip_rows]
-            lse_b = lse_b + q_cum[b : b + 1, lanes[i]]
-            if b == 1:
-                lse_n = jnp.where(upper == 1, t2_l[:, lanes[i]], neg_large)
-                top = jnp.maximum(lse_b, lse_n)
-                w_b, w_n = jnp.exp(lse_b - top), jnp.exp(lse_n - top)
-                tot = w_b + w_n
-                o_b = (o_b * w_b + t2_o[:, lanes[i]] * w_n) / tot
-                lse_b = top + jnp.log(tot)
-            ret_send[b, i] = o_b.astype(bf16)
-            lse_send[b, i] = lse_b
-        for b in range(1, -1, -1):
-
-            @pl.when(z != 2 + b)
-            def _():
-                send_back(
-                    ret_send.at[b, i], ret_recv.at[z, i],
-                    lse_send.at[b, i], lse_recv.at[z, i], i, 2 + b,
-                )
-
-            @pl.when(z == 2 + b)
-            def _():
-                ret_recv[z, i] = ret_send[b, i]
-                lse_recv[z, i] = lse_send[b, i]
-
     def merge(h, slot, i):
         r = pl.ds(h * hd, hd)
         near, far = lse_loc[pl.ds(h, 1), lanes[i]], lse_recv[slot, i]
@@ -625,22 +625,6 @@
         ) / tot
         lse_loc[pl.ds(h, 1), lanes[i]] = top + jnp.log(tot)
 
-    @pl.when(z == 1)
-    def _():
-        settle(ret_recv.at[pl.ds(0, 2)], R["rr"].at[2])
-        settle(lse_recv.at[pl.ds(0, 2)], R["lr"].at[2])
-        for i in range(chips):
-            for h in range(heads):
-                merge(h, h, i)
-
-    @pl.when(z == 3)
-    def _():
-        settle(ret_recv.at[pl.ds(0, 1)], R["rr"].at[2])
-        settle(lse_recv.at[pl.ds(0, 1)], R["lr"].at[2])
-        for i in range(chips):
-            for h in range(2):
-                merge(h, 4 + h, i)
-
     wao_copy.wait()
     cw = d_all // OUT_CHUNKS
     mine = pl.ds(pl.multiple_of(core * own_rows, own_rows), own_rows)
@@ -657,12 +641,14 @@
     def exchange(dist):
         i = chips - 1 - dist
 
-        @pl.when(z > 1)
-        def _():
-            settle(ret_recv.at[pl.ds(0, 3), i], R["rr"].at[i])
-            settle(lse_recv.at[pl.ds(0, 3), i], R["lr"].at[i])
-            for h in range(heads):
-                merge(h, h, i)
+        for zz, n in ((1, 2), (2, 3), (3, 4)):
+
+            @pl.when(z == zz)
+            def _():
+                settle(ret_recv.at[pl.ds(0, n), i], R["rr"].at[i])
+                settle(lse_recv.at[pl.ds(0, n), i], R["lr"].at[i])
+                for slot in range(6 if zz == 3 else heads):
+                    merge(slot % heads, slot, i)
 
         att = out_loc[:, lanes[i]].T.astype(bf16)
         for n in range(OUT_CHUNKS):
@@ -674,6 +660,13 @@
             d_copy(dist, n).start()
 
     exchange(1)
+    for zz, tasks in enumerate(LATE_TASKS):
+        if tasks:
+
+            @pl.when(z == zz)
+            def _():
+                far_part(zz, tasks, {CROSS, SAME, OTHER})
+
     for n in range(OUT_CHUNKS):
         d_copy(1, n).wait_recv()
         x_send[n] = (parts[1, n, mine] + d_recv[1, n].astype(f32)).astype(bf16)
@@ -771,7 +764,8 @@
         "cpart": vm((rows, d_all), f32),
         "t2_o": vm((hd, rows), f32),
         "t2_l": vm((1, rows), f32),
-        "q_cum": vm((2, rows), f32),
+        "s_o": vm((hd, rows), f32),
+        "s_l": vm((1, rows), f32),
         "ret_send": vm((4, chips, hd, 2 * own_rows), bf16),
         "ret_recv": vm((6, chips, hd, 2 * own_rows), bf16),
         "lse_send": vm((4, chips, 1, 2 * own_rows), f32),
@@ -795,8 +789,8 @@
         "st_r": dma,
         "rs": dma,
         "ls": dma,
-        "rr": dma((3,)),
-        "lr": dma((3,)),
+        "rr": dma((chips,)),
+        "lr": dma((chips,)),
         "ds": dma,
         "dr": dma((chips, OUT_CHUNKS)),
         "xs_s": dma,

time: 34 us -> 31.9 us (0.938)
  the two profiles are of different devices: /device:TPU:21 before, /device:TPU:0 now
where the time goes in v2:
time: 31.9 us; the launch traced here: 31.8 us
  Pallas kernels  31.1 us (97%)
  between operations  0.64 us (2%)
    pallas_call x1, Pallas kernels, fused_local(): pl.pallas_call(functools.partial(fused_kernel, n_tp, ARGS + ('out_ref', '...  30.4 us
    pallas_call x1, Pallas kernels, fused_local(): pl.pallas_call(write_out, out_shape=(jax.ShapeDtypeStruct((own_rows, d_al...  0.72 us

profile of v2, /device:TPU:0, one launch (start us, length us, event | category | flops | bytes accessed | tf_op | source)
XLA Modules:
  0.0 31.8 jit_solution(12527215574699531412)
XLA Ops:
  0.6 30.4 %shard_map.131 = (bf16[64,2048]{1,0:T(8,128)(2,1)S(1)}, f32[4,256]{1,0:T(4,128)S(1)}) custom-call(bf16[256,512]{1,0:T(8,128)(2,1)} %refs_0_.1, bf16[2048]{0:T(1024)(128)(2,1)} %refs_1_.1, bf16[256,2048]{1,0:T(8,128)(2,1)} %refs_2_.1, bf16[256,2048]{1,0:T(8,128)(2,1)} %refs_3_.1, bf16[31,256]{1,0:T(8,128)(2,1)} %refs_4_.1, bf16[256]{0:T(256)(128)(2,1)} %refs_5_.1, ...), custom_call_target="tpu_custom_call" | custom-call | tf_op jit(solution)/shard_map/pallas_call | solution.py:801
  31.1 0.7 %shard_map.132 = (bf16[64,2048]{1,0:T(8,128)(2,1)}, f32[4,256]{1,0:T(4,128)}) custom-call(bf16[64,2048]{1,0:T(8,128)(2,1)S(1)} %get-tuple-element.4.m_ref, f32[4,256]{1,0:T(4,128)S(1)} %get-tuple-element.5.l_ref), custom_call_target="tpu_custom_call" | custom-call | tf_op jit(solution)/shard_map/pallas_call | solution.py:814

commit v3 on v2

--- a/solution.py
+++ b/solution.py
@@ -174,14 +174,21 @@
     ((0, Q, 0, CROSS), (1, Q, 1, CROSS), (3, Q, 3, CROSS), (3, KV, 3, SAME), (0, KV, 3, OTHER)),
     ((0, Q, 0, CROSS), (1, Q, 1, CROSS), (2, Q, 2, SAME), (1, Q, 2, OTHER)),
 )
+GREETINGS = (((1,), 0, ()), ((2, 3), 3, (0, 2, 3)), ((1, 3), 2, ()), ((1, 2), 2, ()))
 OTHER_HEAD = (2, 3, 1, 0)
+NORM, FORWARD, ACROSS, BESIDE = 3, 4, 5, 6
 TASKS = (
-    ((CROSS, 0), (SAME, 0), (OTHER, 0)),
-    ((CROSS, 0), (SAME, 0), (OTHER, 0), (CROSS, 1)),
-    ((SAME, 0), (OTHER, 0), (CROSS, 0), (CROSS, 1)),
-    ((SAME, 0), (OTHER, 0), (CROSS, 0), (CROSS, 1)),
+    ((ACROSS, 0), (NORM, 0), (ACROSS, 1), (CROSS, 0), (FORWARD, 0), (SAME, 0), (OTHER, 0),
+     (ACROSS, 2), (ACROSS, 3)),
+    ((ACROSS, 0), (CROSS, 0), (SAME, 0), (ACROSS, 1), (NORM, 0), (OTHER, 0), (ACROSS, 2),
+     (FORWARD, 0), (CROSS, 1), (ACROSS, 3)),
+    ((ACROSS, 0), (SAME, 0), (OTHER, 0), (ACROSS, 1), (NORM, 0), (CROSS, 0), (FORWARD, 0),
+     (ACROSS, 2), (CROSS, 1), (ACROSS, 3)),
+    ((ACROSS, 0), (NORM, 0), (ACROSS, 1), (CROSS, 0), (FORWARD, 0), (SAME, 0), (ACROSS, 2),
+     (OTHER, 0), (CROSS, 1), (ACROSS, 3)),
 )
 LATE_TASKS = (((CROSS, 1),), (), (), ())
+W_PIECES = 4
 ROW_GROUPS = ((3,), (0,), (1, 2))
 
 
@@ -201,12 +208,11 @@
     ext, halo_src, halo, csum = R["ext"], R["halo_src"], R["halo"], R["csum"]
     st_send, st_recv, cpart = R["st_send"], R["st_recv"], R["cpart"]
     t2_o, t2_l, s_o, s_l = R["t2_o"], R["t2_l"], R["s_o"], R["s_l"]
-    ret_send, ret_recv, lse_send, lse_recv = (
-        R["ret_send"], R["ret_recv"], R["lse_send"], R["lse_recv"],
-    )
+    ret_send, ret_recv = R["ret_send"], R["ret_recv"]
     d_send, d_recv, x_send, x_recv, parts = (
         R[n] for n in ("d_send", "d_recv", "x_send", "x_recv", "parts")
     )
+    wall, conv_s, att_s, att_all = R["wall"], R["conv_s"], R["att_s"], R["att_all"]
     ld = R["ld"]
     n_sp = len(ROUTES)
     z = lax.axis_index("sp")
@@ -220,6 +226,7 @@
     hd = attn_w // heads
     d_all = wci_hbm.shape[1]
     partner = chip * 2 + 1 - core
+    grp = lax.axis_index("grp")
 
     def remote(src, dst, s, r, dev):
         return pltpu.make_async_remote_copy(
@@ -247,11 +254,14 @@
         pl.semaphore_signal(
             barrier, inc=1, device_id={"tp": piece_owner(rel)}, device_id_type=MESH
         )
-    for dist in range(1, n_sp):
-        pl.semaphore_signal(
-            barrier, inc=1, device_id={"sp": lax.rem(z + dist, n_sp)}, device_id_type=MESH
-        )
-
+    for src, (greeted, _, _) in enumerate(GREETINGS):
+
+        @pl.when(z == src)
+        def _():
+            for to in greeted:
+                pl.semaphore_signal(barrier, inc=1, device_id={"sp": to}, device_id_type=MESH)
+
+    pl.semaphore_signal(barrier, inc=1, device_id={"grp": 1 - grp}, device_id_type=MESH)
     own_copy = pltpu.make_async_copy(x_hbm, xg.at[0], ld.at[0])
     own_copy.start()
     small = [
@@ -271,11 +281,23 @@
     pltpu.make_async_copy(wci_hbm, wbuf.at[pl.ds(qkv_w, conv_w)], ld.at[2]).start()
     pltpu.make_async_copy(wcg_hbm, wbuf.at[pl.ds(qkv_w + conv_w, conv_w)], ld.at[2]).start()
     wco_copy = pltpu.make_async_copy(R["wco_hbm"], wco, ld.at[3])
-    wao_copy = pltpu.make_async_copy(R["wao_hbm"], wao, ld.at[4])
+    summed = wao.shape[1]
+    wao_copy = pltpu.make_async_copy(R["wao_hbm"].at[:, pl.ds(0, summed)], wao, ld.at[4])
+    wall_copy = pltpu.make_async_copy(
+        R["wao_hbm"].at[:, pl.ds(summed, d_all - summed)], wall.at[0], ld.at[9]
+    )
     wco_copy.start()
     wao_copy.start()
-
-    pl.semaphore_wait(barrier, n_tp - 1 + n_sp - 1)
+    wall_copy.start()
+
+    for src, (_, count, told) in enumerate(GREETINGS):
+
+        @pl.when(z == src)
+        def _():
+            pl.semaphore_wait(barrier, n_tp - 1 + count + 1)
+            for to in told:
+                pl.semaphore_signal(R["ready"], inc=1, device_id={"sp": to}, device_id_type=MESH)
+
 
     rc = rows // AG_CHUNKS
 
@@ -290,12 +312,6 @@
             ag_copy(2 * dist, False, c).start()
     pair_copy = remote(xg.at[0], xg.at[1], R["ag_s"], R["ag_r1"], {"tp": partner})
     pair_copy.start()
-    small[3].wait()
-    for dist in range(1, n_sp):
-        remote(
-            cum_ref, cum_recv.at[z], R["cs"], R["cr"], {"sp": lax.rem(z + dist, n_sp)}
-        ).start()
-    cum_recv[z] = cum_ref[...]
     small[0].wait()
 
     def prepare(rel, c0, n):
@@ -386,8 +402,39 @@
                 xs[2 * dist, r], wcols(2 * dist, 0, qkv_w), NT, preferred_element_type=f32
             )
 
+    w_rows = attn_w // 2 // W_PIECES
+
+    def w_piece(of, p):
+        return pl.ds(pl.multiple_of(of * (attn_w // 2) + p * w_rows, w_rows), w_rows)
+
+    def w_across(p):
+        r = w_piece(grp, p)
+        return remote(
+            wall.at[0, r], wall.at[2, r], R["ws"], R["wx_r"].at[p], {"tp": same_core(1)}
+        )
+
+    def w_beside(p, of):
+        r = w_piece(of, p)
+        return remote(
+            wall.at[2, r], wall.at[2, r], R["ws"], R["wy_r"].at[p], {"grp": 1 - grp}
+        )
+
+    def w_pair(p, of):
+        r = w_piece(of, p)
+        return remote(wall.at[2, r], wall.at[3, r], R["ws"], R["wd_r"], {"tp": partner})
+
     relay(3)
     add_crossed(ROW_GROUPS[0])
+    @pl.when(z != 1)
+    def _():
+        pl.semaphore_wait(R["ready"], 1)
+
+    small[3].wait()
+    for dist in range(1, n_sp):
+        remote(
+            cum_ref, cum_recv.at[z], R["cs"], R["cr"], {"sp": lax.rem(z + dist, n_sp)}
+        ).start()
+    cum_recv[z] = cum_ref[...]
     finish(ROW_GROUPS[0])
     relay(0)
     add_crossed(ROW_GROUPS[1])
@@ -400,11 +447,54 @@
     relay(1)
     finish(ROW_GROUPS[1])
     relay(2)
+    wall_copy.wait()
+    for p in range(W_PIECES // 2):
+        w_across(p).start()
     add_crossed(ROW_GROUPS[2])
     finish(ROW_GROUPS[2])
+    remote(wall.at[0], wall.at[1], R["ws"], R["wp_r"], {"tp": partner}).start()
 
     glu = gated(pl.ds(0, rows))
     ext[rim:, :] = glu.astype(f32)
+    taps = ck_ref.shape[0]
+    blk = 64
+    small[1].wait()
+    small[2].wait()
+
+    def conv_block(b, carry):
+        first = pl.multiple_of(b * blk, blk)
+        block = ext[pl.ds(first, blk + rim), :]
+        tot = jnp.zeros((blk, conv_w), f32)
+        for j in range(taps):
+            off = rim - (taps - 1) + j
+            tot = tot + block[off : off + blk] * ck_ref[j : j + 1, :].astype(f32)
+        csum[pl.ds(first, blk), :] = tot
+        return carry
+
+    lax.fori_loop(1, rows // blk, conv_block, 0)
+
+    @pl.when(z == 0)
+    def _():
+        halo[...] = jnp.zeros_like(halo)
+
+    @pl.when(z > 0)
+    def _():
+        halo_copy.wait_recv()
+
+    ext[:rim, :] = halo[...].astype(f32)
+    conv_block(0, 0)
+    cs = csum[...]
+    first = jnp.sum(cs, axis=1, keepdims=True)
+    second = jnp.sum(cs * cs, axis=1, keepdims=True)
+    lane = lax.broadcasted_iota(jnp.int32, (rows, 128), 1)
+    both = jnp.where(lane == 0, first, second)
+    st_send[...] = both.T[: st_send.shape[0]]
+    for rel in range(1, n_tp):
+        remote(
+            st_send, st_recv.at[rel - 1], R["st_s"], R["st_r"], {"tp": piece_owner(rel)}
+        ).start()
+    for p in range(W_PIECES // 2, W_PIECES):
+        w_across(p).start()
     scale = hd ** (-0.5)
     low = lax.broadcasted_iota(jnp.int32, (rc, 2 * hd), 1) < hd
     wide_k = -(-rows // 128)
@@ -449,43 +539,6 @@
 
     qk_rows = half * 2 * hd * AG_CHUNKS // width
 
-    taps = ck_ref.shape[0]
-    blk = 64
-    small[1].wait()
-    small[2].wait()
-
-    def conv_block(b, carry):
-        first = pl.multiple_of(b * blk, blk)
-        block = ext[pl.ds(first, blk + rim), :]
-        tot = jnp.zeros((blk, conv_w), f32)
-        for j in range(taps):
-            off = rim - (taps - 1) + j
-            tot = tot + block[off : off + blk] * ck_ref[j : j + 1, :].astype(f32)
-        csum[pl.ds(first, blk), :] = tot
-        return carry
-
-    lax.fori_loop(1, rows // blk, conv_block, 0)
-
-    @pl.when(z == 0)
-    def _():
-        halo[...] = jnp.zeros_like(halo)
-
-    @pl.when(z > 0)
-    def _():
-        halo_copy.wait_recv()
-
-    ext[:rim, :] = halo[...].astype(f32)
-    conv_block(0, 0)
-    cs = csum[...]
-    first = jnp.sum(cs, axis=1, keepdims=True)
-    second = jnp.sum(cs * cs, axis=1, keepdims=True)
-    lane = lax.broadcasted_iota(jnp.int32, (rows, 128), 1)
-    both = jnp.where(lane == 0, first, second)
-    st_send[...] = both.T[: st_send.shape[0]]
-    for rel in range(1, n_tp):
-        remote(
-            st_send, st_recv.at[rel - 1], R["st_s"], R["st_r"], {"tp": piece_owner(rel)}
-        ).start()
     settle(cum_recv.at[pl.ds(0, n_sp - 1)], R["cr"])
 
     received = [[0] * 3 for _ in ROUTES]
@@ -500,9 +553,73 @@
         for i in range(chips)
     ]
 
-    def send_back(src_o, dst_o, src_l, dst_l, kind, to):
-        remote(src_o, dst_o, R["rs"], R["rr"].at[kind], {"sp": to}).start()
-        remote(src_l, dst_l, R["ls"], R["lr"].at[kind], {"sp": to}).start()
+    def send_back(send, slot, i, to):
+        remote(
+            ret_send.at[send, i], ret_recv.at[slot, i], R["rs"], R["rr"].at[i], {"sp": to}
+        ).start()
+
+    def fill(ref, o, lse):
+        ref[:hd] = o.astype(bf16)
+        high = lse.astype(bf16)
+        rest = lse - high.astype(f32)
+        mid = rest.astype(bf16)
+        low = rest - mid.astype(f32)
+        row = lax.broadcasted_iota(jnp.int32, (16, lse.shape[1]), 0)
+        terms = jnp.where(row == 0, high.astype(f32), jnp.where(row == 1, mid.astype(f32), low))
+        ref[hd:] = terms.astype(bf16)
+
+    cw = d_all // OUT_CHUNKS
+    early = range(summed // cw, OUT_CHUNKS)
+
+    def owned(tp):
+        return pl.ds(pl.multiple_of(tp * own_rows, own_rows), own_rows)
+
+    def span(n):
+        return slice(n * cw, (n + 1) * cw)
+
+    def d_copy(dist, n):
+        return remote(
+            d_send.at[dist, n], d_recv.at[dist, n], R["ds"], R["dr"].at[dist, n], {"tp": partner}
+        )
+
+    def x_copy(n):
+        return remote(x_send.at[n], x_recv.at[n], R["xs_s"], R["xr"].at[n], {"tp": same_core(1)})
+
+    def conv_norm():
+        settle(st_recv, R["st_r"])
+        tot = st_send[...]
+        for rel in range(1, n_tp):
+            tot = tot + st_recv[rel - 1]
+        wide = jnp.concatenate([tot] * (128 // tot.shape[0]), axis=0).T
+        mean = wide[:, 0:1] / CONV_CH
+        var = wide[:, 1:2] / CONV_CH - mean * mean
+        normed = (
+            (csum[...] - mean)
+            * lax.rsqrt(var + 1e-05)
+            * lng_ref[...].astype(f32).reshape(1, conv_w)
+        )
+        conv_s[...] = (normed / (1.0 + jnp.exp(-normed))).astype(bf16)
+        wco_copy.wait()
+        cpart[...] = jnp.dot(conv_s[...], wco[...], preferred_element_type=f32)
+        for dist, to in ((1, other_core(1)), (0, partner)):
+            for n in early:
+                d_send[dist, n] = cpart[owned(to), span(n)].astype(bf16)
+                d_copy(dist, n).start()
+
+    def conv_forward():
+        for n in early:
+            d_copy(1, n).wait_recv()
+            x_send[n] = (cpart[owned(same_core(1)), span(n)] + d_recv[1, n].astype(f32)).astype(bf16)
+            x_copy(n).start()
+
+    def pass_across(p):
+        w_across(p).wait_recv()
+        w_beside(p, grp).start()
+        w_pair(p, grp).start()
+
+    def pass_beside(p):
+        w_beside(p, 1 - grp).wait_recv()
+        w_pair(p, 1 - grp).start()
 
     def tile(zz, src, h, c):
         if src == zz:
@@ -540,23 +657,21 @@
                     settle(xs.at[0, pl.ds(0, n)], R["zr"].at[kind])
 
         def hand_over(send, slot, i, to, o, lse):
+            fill((ret_recv.at[slot, i] if to == zz else ret_send.at[send, i]), o, lse)
             if to == zz:
-                ret_recv[slot, i] = o.astype(bf16)
-                lse_recv[slot, i] = lse
                 return
-            ret_send[send, i] = o.astype(bf16)
-            lse_send[send, i] = lse
-            args = (
-                ret_send.at[send, i], ret_recv.at[slot, i],
-                lse_send.at[send, i], lse_recv.at[slot, i], i, to,
-            )
             if i == 0:
-                send_back(*args)
+                send_back(send, slot, i, to)
             else:
-                later.append(args)
+                later.append((send, slot, i, to))
 
         for kind, i in tasks:
-            arrived(*((SAME, CROSS) if kind == CROSS else (kind,)))
+            if kind >= NORM:
+                (conv_norm, conv_forward, pass_across, pass_beside)[kind - NORM](
+                    *([i] if kind >= ACROSS else [])
+                )
+                continue
+            arrived(*((SAME, CROSS) if kind == CROSS and zz in (1, 2) else (kind,)))
             if kind == CROSS:
                 if i == 0:
                     far_terms(zz, zz, 0, (0, 1), (2, 3))
@@ -572,7 +687,7 @@
                     o_b = o[:, b * chip_rows : (b + 1) * chip_rows]
                     lse_b = lse[:, b * chip_rows : (b + 1) * chip_rows]
                     lse_b = lse_b + cum_recv[2 + b, zz : zz + 1, lanes[i]]
-                    if b == 1 and upper:
+                    if b == 1 and zz == 2:
                         lse_n = s_l[:, lanes[i]]
                         top = jnp.maximum(lse_b, lse_n)
                         w_b, w_n = jnp.exp(lse_b - top), jnp.exp(lse_n - top)
@@ -584,13 +699,14 @@
             h, r0 = (zz, 2 * rows) if kind == SAME else (OTHER_HEAD[zz], 3 * rows)
             far_terms(zz, h, r0, (key_blk,), (query_blk,))
             o, lse = far_attend(q_s[r0 : r0 + rows], r0, rows)
-            o_ref, l_ref = (s_o, s_l) if kind == SAME else (t2_o, t2_l)
+            o_ref, l_ref = (s_o, s_l) if kind == SAME and zz == 2 else (t2_o, t2_l)
             o_ref[...] = o
             l_ref[...] = lse + cum_recv[query_blk, h : h + 1]
-            if kind == OTHER or not upper:
+            if kind == OTHER or zz != 2:
                 for n in range(chips):
                     hand_over(
-                        kind + 1, h + 4 * upper if kind == OTHER else h, n, query_blk,
+                        kind + 1, 6 if kind == SAME and upper else h + 4 * upper * kind // OTHER,
+                        n, query_blk,
                         o_ref[:, lanes[n]], l_ref[:, lanes[n]],
                     )
         for args in later:
@@ -602,59 +718,49 @@
         def _():
             far_part(zz, TASKS[zz], set())
 
-    settle(st_recv, R["st_r"])
-    tot = st_send[...]
-    for rel in range(1, n_tp):
-        tot = tot + st_recv[rel - 1]
-    wide = jnp.concatenate([tot] * (128 // tot.shape[0]), axis=0).T
-    mean = wide[:, 0:1] / CONV_CH
-    var = wide[:, 1:2] / CONV_CH - mean * mean
-    normed = (csum[...] - mean) * lax.rsqrt(var + 1e-05) * lng_ref[...].astype(f32).reshape(1, conv_w)
-    conv_out = (normed / (1.0 + jnp.exp(-normed))).astype(bf16)
-    wco_copy.wait()
-    cpart[...] = jnp.dot(conv_out, wco[...], preferred_element_type=f32)
-
     def merge(h, slot, i):
         r = pl.ds(h * hd, hd)
-        near, far = lse_loc[pl.ds(h, 1), lanes[i]], lse_recv[slot, i]
+        near, terms = lse_loc[pl.ds(h, 1), lanes[i]], ret_recv[slot, i, hd:].astype(f32)
+        far = terms[0:1] + terms[1:2] + terms[2:3]
         top = jnp.maximum(near, far)
         w_near, w_far = jnp.exp(near - top), jnp.exp(far - top)
         tot = w_near + w_far
         out_loc[r, lanes[i]] = (
-            out_loc[r, lanes[i]] * w_near + ret_recv[slot, i].astype(f32) * w_far
+            out_loc[r, lanes[i]] * w_near + ret_recv[slot, i, :hd].astype(f32) * w_far
         ) / tot
         lse_loc[pl.ds(h, 1), lanes[i]] = top + jnp.log(tot)
 
+    pass_beside(0)
     wao_copy.wait()
-    cw = d_all // OUT_CHUNKS
+    late = range(summed // cw)
     mine = pl.ds(pl.multiple_of(core * own_rows, own_rows), own_rows)
     theirs = pl.ds(pl.multiple_of((1 - core) * own_rows, own_rows), own_rows)
 
-    def d_copy(dist, n):
+    def hand_rows(i, r, rel, to):
         return remote(
-            d_send.at[dist, n], d_recv.at[dist, n], R["ds"], R["dr"].at[dist, n], {"tp": partner}
+            att_s.at[i, r], att_all.at[rel], R["at_s"], R["at_r"].at[rel // 2], {"tp": to}
         )
-
-    def x_copy(n):
-        return remote(x_send.at[n], x_recv.at[n], R["xs_s"], R["xr"].at[n], {"tp": same_core(1)})
 
     def exchange(dist):
         i = chips - 1 - dist
-
         for zz, n in ((1, 2), (2, 3), (3, 4)):
 
             @pl.when(z == zz)
             def _():
                 settle(ret_recv.at[pl.ds(0, n), i], R["rr"].at[i])
-                settle(lse_recv.at[pl.ds(0, n), i], R["lr"].at[i])
-                for slot in range(6 if zz == 3 else heads):
-                    merge(slot % heads, slot, i)
+                for slot in range(7 if zz == 3 else heads):
+                    merge(3 if slot == 6 else slot % heads, slot, i)
 
         att = out_loc[:, lanes[i]].T.astype(bf16)
-        for n in range(OUT_CHUNKS):
-            cols = slice(n * cw, (n + 1) * cw)
-            parts[dist, n] = cpart[lanes[i], cols] + jnp.dot(
-                att, wao[:, cols], preferred_element_type=f32
+        att_s[i] = att
+        if dist:
+            hand_rows(i, mine, 2, same_core(1)).start()
+            hand_rows(i, theirs, 3, other_core(1)).start()
+        else:
+            hand_rows(i, theirs, 1, partner).start()
+        for n in late:
+            parts[dist, n] = cpart[lanes[i], span(n)] + jnp.dot(
+                att, wao[:, span(n)], preferred_element_type=f32
             )
             d_send[dist, n] = parts[dist, n, theirs].astype(bf16)
             d_copy(dist, n).start()
@@ -667,19 +773,37 @@
             def _():
                 far_part(zz, tasks, {CROSS, SAME, OTHER})
 
-    for n in range(OUT_CHUNKS):
+    for n in late:
         d_copy(1, n).wait_recv()
         x_send[n] = (parts[1, n, mine] + d_recv[1, n].astype(f32)).astype(bf16)
         x_copy(n).start()
     exchange(0)
     log_ref[...] = lse_loc[...]
-    for n in range(OUT_CHUNKS):
+    for p in range(1, W_PIECES):
+        pass_beside(p)
+    settle(wall.at[1], R["wp_r"])
+    whole = jnp.dot(att_s[1, mine], wall[0], preferred_element_type=f32)
+    settle(att_all.at[1], R["at_r"].at[0])
+    whole = whole + jnp.dot(att_all[1], wall[1], preferred_element_type=f32)
+    settle(att_all.at[pl.ds(2, 2)], R["at_r"].at[1])
+    whole = whole + jnp.dot(att_all[2], wall[2], preferred_element_type=f32)
+    settle(wall.at[3], R["wd_r"])
+    whole = whole + jnp.dot(att_all[3], wall[3], preferred_element_type=f32)
+    for n in early:
+        d_copy(0, n).wait_recv()
+        x_copy(n).wait_recv()
+        tot = whole[:, n * cw - summed : (n + 1) * cw - summed] + cpart[owned(me), span(n)]
+        tot = tot + d_recv[0, n].astype(f32) + x_recv[n].astype(f32)
+        out_ref[:, span(n)] = tot.astype(bf16)
+    for n in late:
         d_copy(0, n).wait_recv()
         tot = parts[0, n, mine] + d_recv[0, n].astype(f32)
         x_copy(n).wait_recv()
         tot = tot + x_recv[n].astype(f32)
-        out_ref[:, n * cw : (n + 1) * cw] = tot.astype(bf16)
-
+        out_ref[:, span(n)] = tot.astype(bf16)
+
+    settle(wall.at[pl.ds(0, 3)], R["ws"])
+    settle(att_all.at[pl.ds(0, 3)], R["at_s"])
     settle(xg.at[pl.ds(1, n_tp - 1)], R["ag_s"])
     settle(cum_recv.at[pl.ds(0, n_sp - 1)], R["cs"])
     settle(st_recv, R["st_s"])
@@ -697,7 +821,6 @@
         def _():
             settle(xs.at[0, pl.ds(0, n * qk_rows)], R["zs"])
             settle(ret_recv.at[pl.ds(0, back)], R["rs"])
-            settle(lse_recv.at[pl.ds(0, back)], R["ls"])
 
 
 def write_out(m_ref, l_ref, m_hbm, l_hbm, sem):
@@ -737,7 +860,11 @@
         "xs": vm((n_tp, rows, width), bf16),
         "wbuf": vm((all_w, d_all), bf16),
         "wco": vm((conv_w, d_all), bf16),
-        "wao": vm((attn_w, d_all), bf16),
+        "wao": vm((attn_w, d_all // 2), bf16),
+        "wall": vm((n_tp, attn_w, d_all // 2), bf16),
+        "conv_s": vm((rows, conv_w), bf16),
+        "att_s": vm((chips, 2 * own_rows, attn_w), bf16),
+        "att_all": vm((n_tp, own_rows, attn_w), bf16),
         "gain": vm(norm_gain.shape, bf16),
         "ck": vm(conv_kernel.shape, bf16),
         "lng": vm(ln_gain.shape, bf16),
@@ -766,16 +893,22 @@
         "t2_l": vm((1, rows), f32),
         "s_o": vm((hd, rows), f32),
         "s_l": vm((1, rows), f32),
-        "ret_send": vm((4, chips, hd, 2 * own_rows), bf16),
-        "ret_recv": vm((6, chips, hd, 2 * own_rows), bf16),
-        "lse_send": vm((4, chips, 1, 2 * own_rows), f32),
-        "lse_recv": vm((6, chips, 1, 2 * own_rows), f32),
+        "ret_send": vm((4, chips, hd + 16, 2 * own_rows), bf16),
+        "ret_recv": vm((7, chips, hd + 16, 2 * own_rows), bf16),
         "d_send": vm((chips, OUT_CHUNKS, own_rows, cw), bf16),
         "d_recv": vm((chips, OUT_CHUNKS, own_rows, cw), bf16),
         "x_send": vm((OUT_CHUNKS, own_rows, cw), bf16),
         "x_recv": vm((OUT_CHUNKS, own_rows, cw), bf16),
-        "parts": vm((chips, OUT_CHUNKS, 2 * own_rows, cw), f32),
-        "ld": dma((9,)),
+        "parts": vm((chips, OUT_CHUNKS // 2, 2 * own_rows, cw), f32),
+        "ld": dma((10,)),
+        "ws": dma,
+        "wp_r": dma,
+        "wd_r": dma,
+        "wx_r": dma((W_PIECES,)),
+        "wy_r": dma((W_PIECES,)),
+        "at_s": dma,
+        "at_r": dma((2,)),
+        "ready": pltpu.SemaphoreType.REGULAR,
         "ag_s": dma,
         "ag_r1": dma,
         "ag_r": dma((n_tp - 2, AG_CHUNKS)),
@@ -788,9 +921,7 @@
         "st_s": dma,
         "st_r": dma,
         "rs": dma,
-        "ls": dma,
         "rr": dma((chips,)),
-        "lr": dma((chips,)),
         "ds": dma,
         "dr": dma((chips, OUT_CHUNKS)),
         "xs_s": dma,
@@ -841,5 +972,6 @@
     out_specs = (P(("grp", "sp", "tp"), None), P("tp", ("grp", "sp")))
     heads_here = HEADS // mesh.shape["tp"]
     fits = heads_here == mesh.shape["sp"] == len(ROUTES) and mesh.shape["tp"] == 4
+    fits = fits and mesh.shape["grp"] == 2
     body = functools.partial(fused_local, mesh.shape["tp"]) if fits else local
     return jax.shard_map(body, mesh=mesh, in_specs=in_specs, out_specs=out_specs, check_vma=False)

time: 31.9 us -> 30.3 us (0.950)
  Pallas kernels: 31.1 us -> 29.4 us
    pallas_call x1, Pallas kernels: 30.4 us -> 28.6 us  [fused_local(): pl.pallas_call(functools.partial(fused_kernel, n_tp, ARGS + ('out_ref', '...]
where the time goes in v3:
time: 30.3 us; the launch traced here: 30.2 us
  Pallas kernels  29.4 us (97%)
  between operations  0.8 us (3%)
    pallas_call x1, Pallas kernels, fused_local(): pl.pallas_call(functools.partial(fused_kernel, n_tp, ARGS + ('out_ref', '...  28.6 us
    pallas_call x1, Pallas kernels, fused_local(): pl.pallas_call(write_out, out_shape=(jax.ShapeDtypeStruct((own_rows, d_al...  0.72 us

profile of v3, /device:TPU:0, one launch (start us, length us, event | category | flops | bytes accessed | tf_op | source)
XLA Modules:
  0.0 30.2 jit_solution(11868004091022344370)
XLA Ops:
  0.6 28.6 %shard_map.131 = (bf16[64,2048]{1,0:T(8,128)(2,1)S(1)}, f32[4,256]{1,0:T(4,128)S(1)}) custom-call(bf16[256,512]{1,0:T(8,128)(2,1)} %refs_0_.1, bf16[2048]{0:T(1024)(128)(2,1)} %refs_1_.1, bf16[256,2048]{1,0:T(8,128)(2,1)} %refs_2_.1, bf16[256,2048]{1,0:T(8,128)(2,1)} %refs_3_.1, bf16[31,256]{1,0:T(8,128)(2,1)} %refs_4_.1, bf16[256]{0:T(256)(128)(2,1)} %refs_5_.1, ...), custom_call_target="tpu_custom_call" | custom-call | tf_op jit(solution)/shard_map/pallas_call | solution.py:932
  29.3 0.7 %shard_map.132 = (bf16[64,2048]{1,0:T(8,128)(2,1)}, f32[4,256]{1,0:T(4,128)}) custom-call(bf16[64,2048]{1,0:T(8,128)(2,1)S(1)} %get-tuple-element.4.m_ref, f32[4,256]{1,0:T(4,128)S(1)} %get-tuple-element.5.l_ref), custom_call_target="tpu_custom_call" | custom-call | tf_op jit(solution)/shard_map/pallas_call | solution.py:945

commit v4 on v3

--- a/solution.py
+++ b/solution.py
@@ -163,7 +163,7 @@
 
 
 AG_CHUNKS = 4
-OUT_CHUNKS = 4
+SUMMED_EIGHTHS = 3
 MESH = pl.DeviceIdType.MESH
 NT = (((1,), (1,)), ((), ()))
 KV, Q = 0, 1
@@ -176,18 +176,17 @@
 )
 GREETINGS = (((1,), 0, ()), ((2, 3), 3, (0, 2, 3)), ((1, 3), 2, ()), ((1, 2), 2, ()))
 OTHER_HEAD = (2, 3, 1, 0)
-NORM, FORWARD, ACROSS, BESIDE = 3, 4, 5, 6
+NORM, FORWARD, SUMS, ACROSS, EXCHANGE = 3, 4, 5, 6, 7
 TASKS = (
-    ((ACROSS, 0), (NORM, 0), (ACROSS, 1), (CROSS, 0), (FORWARD, 0), (SAME, 0), (OTHER, 0),
-     (ACROSS, 2), (ACROSS, 3)),
-    ((ACROSS, 0), (CROSS, 0), (SAME, 0), (ACROSS, 1), (NORM, 0), (OTHER, 0), (ACROSS, 2),
-     (FORWARD, 0), (CROSS, 1), (ACROSS, 3)),
+    ((ACROSS, 0), (NORM, 0), (EXCHANGE, 1), (ACROSS, 1), (CROSS, 0), (FORWARD, 0), (OTHER, 0),
+     (SAME, 0), (SUMS, 0), (ACROSS, 2), (ACROSS, 3), (OTHER, 1), (SAME, 1), (CROSS, 1)),
+    ((ACROSS, 0), (CROSS, 0), (NORM, 0), (ACROSS, 1), (SAME, 0), (FORWARD, 0), (OTHER, 0),
+     (ACROSS, 2), (CROSS, 1), (ACROSS, 3)),
     ((ACROSS, 0), (SAME, 0), (OTHER, 0), (ACROSS, 1), (NORM, 0), (CROSS, 0), (FORWARD, 0),
      (ACROSS, 2), (CROSS, 1), (ACROSS, 3)),
     ((ACROSS, 0), (NORM, 0), (ACROSS, 1), (CROSS, 0), (FORWARD, 0), (SAME, 0), (ACROSS, 2),
      (OTHER, 0), (CROSS, 1), (ACROSS, 3)),
 )
-LATE_TASKS = (((CROSS, 1),), (), (), ())
 W_PIECES = 4
 ROW_GROUPS = ((3,), (0,), (1, 2))
 
@@ -209,10 +208,11 @@
     st_send, st_recv, cpart = R["st_send"], R["st_recv"], R["cpart"]
     t2_o, t2_l, s_o, s_l = R["t2_o"], R["t2_l"], R["s_o"], R["s_l"]
     ret_send, ret_recv = R["ret_send"], R["ret_recv"]
-    d_send, d_recv, x_send, x_recv, parts = (
-        R[n] for n in ("d_send", "d_recv", "x_send", "x_recv", "parts")
-    )
-    wall, conv_s, att_s, att_all = R["wall"], R["conv_s"], R["att_s"], R["att_all"]
+    d_send, d_recv, x_send, x_recv = (
+        [R[f"{name}{n}"] for n in range(4)] for name in ("d_send", "d_recv", "x_send", "x_recv")
+    )
+    parts = R["parts"]
+    wall, stat_s, att_s, att_all = R["wall"], R["stat_s"], R["att_s"], R["att_all"]
     ld = R["ld"]
     n_sp = len(ROUTES)
     z = lax.axis_index("sp")
@@ -568,48 +568,50 @@
         terms = jnp.where(row == 0, high.astype(f32), jnp.where(row == 1, mid.astype(f32), low))
         ref[hd:] = terms.astype(bf16)
 
-    cw = d_all // OUT_CHUNKS
-    early = range(summed // cw, OUT_CHUNKS)
+    late, early = range(2), range(2, 4)
 
     def owned(tp):
         return pl.ds(pl.multiple_of(tp * own_rows, own_rows), own_rows)
 
-    def span(n):
-        return slice(n * cw, (n + 1) * cw)
+    def span(n, base=0):
+        w = (d_all - summed) // 2 if n in early else summed // 2
+        first = (summed if n in early else 0) + n % 2 * w - base
+        return slice(first, first + w)
 
     def d_copy(dist, n):
         return remote(
-            d_send.at[dist, n], d_recv.at[dist, n], R["ds"], R["dr"].at[dist, n], {"tp": partner}
+            d_send[n].at[dist], d_recv[n].at[dist], R["ds"].at[n], R["dr"].at[dist, n],
+            {"tp": partner},
         )
 
     def x_copy(n):
-        return remote(x_send.at[n], x_recv.at[n], R["xs_s"], R["xr"].at[n], {"tp": same_core(1)})
+        return remote(x_send[n], x_recv[n], R["xs_s"].at[n], R["xr"].at[n], {"tp": same_core(1)})
 
     def conv_norm():
         settle(st_recv, R["st_r"])
         tot = st_send[...]
         for rel in range(1, n_tp):
             tot = tot + st_recv[rel - 1]
-        wide = jnp.concatenate([tot] * (128 // tot.shape[0]), axis=0).T
-        mean = wide[:, 0:1] / CONV_CH
-        var = wide[:, 1:2] / CONV_CH - mean * mean
-        normed = (
-            (csum[...] - mean)
-            * lax.rsqrt(var + 1e-05)
-            * lng_ref[...].astype(f32).reshape(1, conv_w)
-        )
-        conv_s[...] = (normed / (1.0 + jnp.exp(-normed))).astype(bf16)
+        stat_s[...] = jnp.concatenate([tot] * (128 // tot.shape[0]), axis=0).T
+        gain = lng_ref[...].astype(f32).reshape(1, conv_w)
         wco_copy.wait()
-        cpart[...] = jnp.dot(conv_s[...], wco[...], preferred_element_type=f32)
-        for dist, to in ((1, other_core(1)), (0, partner)):
+        wao_copy.wait()
+        for i, (dist, to) in enumerate(((1, other_core(1)), (0, partner))):
+            mean = stat_s[lanes[i], 0:1] / CONV_CH
+            var = stat_s[lanes[i], 1:2] / CONV_CH - mean * mean
+            normed = (csum[lanes[i]] - mean) * lax.rsqrt(var + 1e-05) * gain
+            conv_out = (normed / (1.0 + jnp.exp(-normed))).astype(bf16)
+            cpart[lanes[i]] = jnp.dot(conv_out, wco[...], preferred_element_type=f32)
             for n in early:
-                d_send[dist, n] = cpart[owned(to), span(n)].astype(bf16)
+                d_send[n][dist] = cpart[owned(to), span(n)].astype(bf16)
                 d_copy(dist, n).start()
 
     def conv_forward():
         for n in early:
             d_copy(1, n).wait_recv()
-            x_send[n] = (cpart[owned(same_core(1)), span(n)] + d_recv[1, n].astype(f32)).astype(bf16)
+            x_send[n][...] = (
+                cpart[owned(same_core(1)), span(n)] + d_recv[n][1].astype(f32)
+            ).astype(bf16)
             x_copy(n).start()
 
     def pass_across(p):
@@ -641,7 +643,7 @@
 
     def far_attend(q, r0, n_k):
         keys = slice(r0, r0 + n_k)
-        cum_k = jnp.concatenate([cum_col[keys]] * wide_k, axis=1)
+        cum_k = jnp.concatenate([cum_col[keys]] * (q.shape[0] // 128), axis=1)
         return attend(q, k_s[keys], v_t[:, keys], cum_k, False)
 
     def far_part(zz, tasks, seen):
@@ -667,7 +669,7 @@
 
         for kind, i in tasks:
             if kind >= NORM:
-                (conv_norm, conv_forward, pass_across, pass_beside)[kind - NORM](
+                (conv_norm, conv_forward, sum_forward, pass_across, exchange)[kind - NORM](
                     *([i] if kind >= ACROSS else [])
                 )
                 continue
@@ -697,7 +699,14 @@
                     hand_over(b, zz, i, 2 + b, o_b, lse_b)
                 continue
             h, r0 = (zz, 2 * rows) if kind == SAME else (OTHER_HEAD[zz], 3 * rows)
-            far_terms(zz, h, r0, (key_blk,), (query_blk,))
+            if i == 0:
+                far_terms(zz, h, r0, (key_blk,), (query_blk,))
+            if zz == 0:
+                q = q_s[pl.ds(pl.multiple_of(r0 + lanes[i].start, chip_rows), chip_rows)]
+                o, lse = far_attend(q, r0, rows)
+                lse = lse + cum_recv[query_blk, h : h + 1, lanes[i]]
+                hand_over(kind + 1, h, i, query_blk, o, lse)
+                continue
             o, lse = far_attend(q_s[r0 : r0 + rows], r0, rows)
             o_ref, l_ref = (s_o, s_l) if kind == SAME and zz == 2 else (t2_o, t2_l)
             o_ref[...] = o
@@ -712,12 +721,6 @@
         for args in later:
             send_back(*args)
 
-    for zz in range(n_sp):
-
-        @pl.when(z == zz)
-        def _():
-            far_part(zz, TASKS[zz], set())
-
     def merge(h, slot, i):
         r = pl.ds(h * hd, hd)
         near, terms = lse_loc[pl.ds(h, 1), lanes[i]], ret_recv[slot, i, hd:].astype(f32)
@@ -730,9 +733,6 @@
         ) / tot
         lse_loc[pl.ds(h, 1), lanes[i]] = top + jnp.log(tot)
 
-    pass_beside(0)
-    wao_copy.wait()
-    late = range(summed // cw)
     mine = pl.ds(pl.multiple_of(core * own_rows, own_rows), own_rows)
     theirs = pl.ds(pl.multiple_of((1 - core) * own_rows, own_rows), own_rows)
 
@@ -762,21 +762,28 @@
             parts[dist, n] = cpart[lanes[i], span(n)] + jnp.dot(
                 att, wao[:, span(n)], preferred_element_type=f32
             )
-            d_send[dist, n] = parts[dist, n, theirs].astype(bf16)
+            d_send[n][dist] = parts[dist, n, theirs].astype(bf16)
             d_copy(dist, n).start()
 
-    exchange(1)
-    for zz, tasks in enumerate(LATE_TASKS):
-        if tasks:
-
-            @pl.when(z == zz)
-            def _():
-                far_part(zz, tasks, {CROSS, SAME, OTHER})
-
-    for n in late:
-        d_copy(1, n).wait_recv()
-        x_send[n] = (parts[1, n, mine] + d_recv[1, n].astype(f32)).astype(bf16)
-        x_copy(n).start()
+    def sum_forward():
+        for n in late:
+            d_copy(1, n).wait_recv()
+            x_send[n][...] = (parts[1, n, mine] + d_recv[n][1].astype(f32)).astype(bf16)
+            x_copy(n).start()
+
+    for zz in range(n_sp):
+
+        @pl.when(z == zz)
+        def _():
+            far_part(zz, TASKS[zz], set())
+
+    pass_beside(0)
+
+    @pl.when(z > 0)
+    def _():
+        exchange(1)
+        sum_forward()
+
     exchange(0)
     log_ref[...] = lse_loc[...]
     for p in range(1, W_PIECES):
@@ -792,14 +799,14 @@
     for n in early:
         d_copy(0, n).wait_recv()
         x_copy(n).wait_recv()
-        tot = whole[:, n * cw - summed : (n + 1) * cw - summed] + cpart[owned(me), span(n)]
-        tot = tot + d_recv[0, n].astype(f32) + x_recv[n].astype(f32)
+        tot = whole[:, span(n, summed)] + cpart[owned(me), span(n)]
+        tot = tot + d_recv[n][0].astype(f32) + x_recv[n][...].astype(f32)
         out_ref[:, span(n)] = tot.astype(bf16)
     for n in late:
         d_copy(0, n).wait_recv()
-        tot = parts[0, n, mine] + d_recv[0, n].astype(f32)
+        tot = parts[0, n, mine] + d_recv[n][0].astype(f32)
         x_copy(n).wait_recv()
-        tot = tot + x_recv[n].astype(f32)
+        tot = tot + x_recv[n][...].astype(f32)
         out_ref[:, span(n)] = tot.astype(bf16)
 
     settle(wall.at[pl.ds(0, 3)], R["ws"])
@@ -807,8 +814,9 @@
     settle(xg.at[pl.ds(1, n_tp - 1)], R["ag_s"])
     settle(cum_recv.at[pl.ds(0, n_sp - 1)], R["cs"])
     settle(st_recv, R["st_s"])
-    settle(d_send, R["ds"])
-    settle(x_send, R["xs_s"])
+    for n in range(4):
+        settle(d_send[n], R["ds"].at[n])
+        settle(x_send[n], R["xs_s"].at[n])
 
     @pl.when(z < n_sp - 1)
     def _():
@@ -851,7 +859,8 @@
     own_rows = rows // n_tp
     rc = rows // AG_CHUNKS
     rim = -(-(conv_kernel.shape[0] - 1) // 16) * 16
-    cw = d_all // OUT_CHUNKS
+    summed = d_all * SUMMED_EIGHTHS // 8
+    widths = [summed // 2] * 2 + [(d_all - summed) // 2] * 2
     all_w = 3 * attn_w + 2 * conv_w
     dma = pltpu.SemaphoreType.DMA
     vm = pltpu.VMEM
@@ -860,9 +869,9 @@
         "xs": vm((n_tp, rows, width), bf16),
         "wbuf": vm((all_w, d_all), bf16),
         "wco": vm((conv_w, d_all), bf16),
-        "wao": vm((attn_w, d_all // 2), bf16),
-        "wall": vm((n_tp, attn_w, d_all // 2), bf16),
-        "conv_s": vm((rows, conv_w), bf16),
+        "wao": vm((attn_w, summed), bf16),
+        "wall": vm((n_tp, attn_w, d_all - summed), bf16),
+        "stat_s": vm((rows, 128), f32),
         "att_s": vm((chips, 2 * own_rows, attn_w), bf16),
         "att_all": vm((n_tp, own_rows, attn_w), bf16),
         "gain": vm(norm_gain.shape, bf16),
@@ -895,11 +904,11 @@
         "s_l": vm((1, rows), f32),
         "ret_send": vm((4, chips, hd + 16, 2 * own_rows), bf16),
         "ret_recv": vm((7, chips, hd + 16, 2 * own_rows), bf16),
-        "d_send": vm((chips, OUT_CHUNKS, own_rows, cw), bf16),
-        "d_recv": vm((chips, OUT_CHUNKS, own_rows, cw), bf16),
-        "x_send": vm((OUT_CHUNKS, own_rows, cw), bf16),
-        "x_recv": vm((OUT_CHUNKS, own_rows, cw), bf16),
-        "parts": vm((chips, OUT_CHUNKS // 2, 2 * own_rows, cw), f32),
+        **{f"d_send{n}": vm((chips, own_rows, w), bf16) for n, w in enumerate(widths)},
+        **{f"d_recv{n}": vm((chips, own_rows, w), bf16) for n, w in enumerate(widths)},
+        **{f"x_send{n}": vm((own_rows, w), bf16) for n, w in enumerate(widths)},
+        **{f"x_recv{n}": vm((own_rows, w), bf16) for n, w in enumerate(widths)},
+        "parts": vm((chips, 2, 2 * own_rows, summed // 2), f32),
         "ld": dma((10,)),
         "ws": dma,
         "wp_r": dma,
@@ -922,10 +931,10 @@
         "st_r": dma,
         "rs": dma,
         "rr": dma((chips,)),
-        "ds": dma,
-        "dr": dma((chips, OUT_CHUNKS)),
-        "xs_s": dma,
-        "xr": dma((OUT_CHUNKS,)),
+        "ds": dma((4,)),
+        "dr": dma((chips, 4)),
+        "xs_s": dma((4,)),
+        "xr": dma((4,)),
     }
     far = pl.BlockSpec(memory_space=pl.ANY)
     near = pl.BlockSpec(memory_space=pltpu.VMEM)

time: 30.3 us -> 29.8 us (0.983)
  Pallas kernels: 29.4 us -> 28.9 us
    pallas_call x1, Pallas kernels: 28.6 us -> 28.2 us  [fused_local(): pl.pallas_call(functools.partial(fused_kernel, n_tp, ARGS + ('out_ref', '...]
where the time goes in v4:
time: 29.8 us; the launch traced here: 29.7 us
  Pallas kernels  28.9 us (97%)
  between operations  0.8 us (3%)
    pallas_call x1, Pallas kernels, fused_local(): pl.pallas_call(functools.partial(fused_kernel, n_tp, ARGS + ('out_ref', '...  28.2 us
    pallas_call x1, Pallas kernels, fused_local(): pl.pallas_call(write_out, out_shape=(jax.ShapeDtypeStruct((own_rows, d_al...  0.72 us

profile of v4, /device:TPU:0, one launch (start us, length us, event | category | flops | bytes accessed | tf_op | source)
XLA Modules:
  0.0 29.7 jit_solution(6956419453123735927)
XLA Ops:
  0.6 28.2 %shard_map.131 = (bf16[64,2048]{1,0:T(8,128)(2,1)S(1)}, f32[4,256]{1,0:T(4,128)S(1)}) custom-call(bf16[256,512]{1,0:T(8,128)(2,1)} %refs_0_.1, bf16[2048]{0:T(1024)(128)(2,1)} %refs_1_.1, bf16[256,2048]{1,0:T(8,128)(2,1)} %refs_2_.1, bf16[256,2048]{1,0:T(8,128)(2,1)} %refs_3_.1, bf16[31,256]{1,0:T(8,128)(2,1)} %refs_4_.1, bf16[256]{0:T(256)(128)(2,1)} %refs_5_.1, ...), custom_call_target="tpu_custom_call" | custom-call | tf_op jit(solution)/shard_map/pallas_call | solution.py:941
  28.8 0.7 %shard_map.132 = (bf16[64,2048]{1,0:T(8,128)(2,1)}, f32[4,256]{1,0:T(4,128)}) custom-call(bf16[64,2048]{1,0:T(8,128)(2,1)S(1)} %get-tuple-element.4.m_ref, f32[4,256]{1,0:T(4,128)S(1)} %get-tuple-element.5.l_ref), custom_call_target="tpu_custom_call" | custom-call | tf_op jit(solution)/shard_map/pallas_call | solution.py:954
